TPU v7x, 32 devices: a whole 2x2x4 slice. The times are simulated.
32 devices in a mesh: fs: 4 (over y, x), tp: 8 (over z, core).
Axes of the slice: x: 2, y: 2, z: 4, core: 2. Of those that a mesh axis runs over, the one named last changes fastest.
Arguments:
- tokens: bfloat16 [4096, 2048], P(('fs', 'tp')), may hold values from -6 to 6
- gate_weight: bfloat16 [2048, 5632], P('fs', 'tp'), may hold values from -0.125 to 0.125
- up_weight: bfloat16 [2048, 5632], P('fs', 'tp'), may hold values from -0.125 to 0.125
- down_weight: bfloat16 [5632, 2048], P('tp', 'fs'), may hold values from -0.078125 to 0.078125
- grad_out: bfloat16 [4096, 2048], P(('fs', 'tp')), may hold values from -6 to 6
Outputs:
- grad_input: bfloat16 [4096, 2048], P(('fs', 'tp'))
- grad_gate: float32 [2048, 5632], P('fs', 'tp')
- grad_up: float32 [2048, 5632], P('fs', 'tp')
- grad_down: float32 [5632, 2048], P('tp', 'fs')
All inputs are finite; a program needn't handle non-finite values.
Results may differ from a plain program's by a relative error of at most 0.0049.
Values may be sent and summed in bfloat16 or wider, within the bound.
A program may use at most 128 MiB of HBM per device.

v0:
```python
import functools

import jax
import jax.numpy as jnp
from jax import lax
from jax.experimental import pallas as pl
from jax.experimental.pallas import tpu as pltpu
from jax.sharding import PartitionSpec as P

MESH = pl.DeviceIdType.MESH
CORES = 2


def over_rows(left, right, out=jnp.float32):
    return lax.dot_general(
        left, right, (((0,), (0,)), ((), ())), preferred_element_type=jnp.float32
    ).astype(out)


def over_cols(left, right):
    return lax.dot_general(
        left, right, (((1,), (1,)), ((), ())), preferred_element_type=jnp.float32
    )


def orders_of(n_fs):
    bits = [1 << i for i in range(n_fs.bit_length() - 1)]
    return (bits, bits[::-1])


def first_bit(order, mask):
    return next(i for i, bit in enumerate(order) if mask & bit)


def greet(n_fs, depth, fs, tp, z):
    barrier = pltpu.get_barrier_semaphore()
    bits = orders_of(n_fs)[0]

    def hello(fs_id, tp_id):
        pl.semaphore_signal(barrier, inc=1, device_id=(fs_id, tp_id), device_id_type=MESH)

    for bit in bits:
        hello(fs ^ bit, tp)
    hello(fs, tp ^ 1)

    @pl.when(z > 0)
    def _():
        hello(fs, tp - CORES)

    @pl.when(z < depth - 1)
    def _():
        hello(fs, tp + CORES)

    ends = (z > 0).astype(jnp.int32) + (z < depth - 1).astype(jnp.int32)
    pl.semaphore_wait(barrier, len(bits) + 1 + ends)


def gather_kernel(n_fs, n_tp, *refs):
    ins, outs = refs[:5], refs[5:10]
    w_send, w_recv, z_send, z_recv, c_send, c_recv, l_sem = refs[10:]
    fs, tp = lax.axis_index("fs"), lax.axis_index("tp")
    depth = n_tp // CORES
    z = tp // CORES
    orders = orders_of(n_fs)
    phases = len(orders[0])
    weights = tuple((ins[i], outs[i]) for i in (1, 2, 3))
    rows = ((ins[0], outs[0]), (ins[4], outs[4]))
    greet(n_fs, depth, fs, tp, z)

    def w_block(array, split, owner):
        ref, out = weights[array]
        half, cols = ref.shape[0] // 2, ref.shape[1]
        own = ref.at[pl.ds(split * half, half), :]
        there = out.at[pl.ds(split * half, half), pl.ds(pl.multiple_of(owner * cols, cols), cols)]
        return own, there

    def w_copy(array, split, phase, mask):
        own, there = w_block(array, split, fs ^ mask)
        order = orders[split]
        slot = (array, split, (1 << phase) - 1 + sum(1 << i for i in range(phase) if mask & order[i]))
        return pltpu.make_async_remote_copy(
            src_ref=own if mask == 0 else there,
            dst_ref=there,
            send_sem=w_send.at[slot],
            recv_sem=w_recv.at[slot],
            device_id=(fs ^ order[phase], tp),
            device_id_type=MESH,
        )

    def r_block(array, owner):
        ref, out = rows[array]
        n = ref.shape[0]
        return out.at[pl.ds(pl.multiple_of(owner * n, n), n), :]

    def z_copy(array, way, step):
        sign = 1 if way == 0 else -1
        there = r_block(array, tp - sign * step * CORES)
        return pltpu.make_async_remote_copy(
            src_ref=rows[array][0] if step == 0 else there,
            dst_ref=there,
            send_sem=z_send.at[array, way, step],
            recv_sem=z_recv.at[array, way, step],
            device_id=(fs, tp + sign * CORES),
            device_id_type=MESH,
        )

    def sends(way, step):
        if way == 0:
            return jnp.logical_and(z - step >= 0, z < depth - 1)
        return jnp.logical_and(z + step <= depth - 1, z > 0)

    def arrives(way, step):
        return z - 1 - step >= 0 if way == 0 else z + 1 + step <= depth - 1

    def c_copy(array, way, step):
        sign = 1 if way == 0 else -1
        there = r_block(array, tp - sign * (step + 1) * CORES)
        slot = (array, way, step + 1)
        return pltpu.make_async_remote_copy(
            src_ref=rows[array][0] if step == -1 else there,
            dst_ref=there,
            send_sem=c_send.at[slot],
            recv_sem=c_recv.at[slot],
            device_id=(fs, tp ^ 1),
            device_id_type=MESH,
        )

    for array in range(2):
        for way in range(2):

            @pl.when(sends(way, 0))
            def _():
                z_copy(array, way, 0).start()

    for phase in range(phases):
        for array in range(3):
            for split in range(2):
                w_copy(array, split, phase, 0).start()
    for array in range(2):
        c_copy(array, 0, -1).start()
    local = []
    for array in range(3):
        for split in range(2):
            own, there = w_block(array, split, fs)
            local.append((own, there))
    for array in range(2):
        local.append((rows[array][0], r_block(array, tp)))
    local = [pltpu.make_async_copy(a, b, l_sem.at[i]) for i, (a, b) in enumerate(local)]
    for copy in local:
        copy.start()

    def w_event(array, phase, index):
        for split in range(2):
            order = orders[split]
            mask = sum(order[i] for i in range(phase) if index & (1 << i))
            w_copy(array, split, phase, mask).wait_recv()
            got = mask | order[phase]
            for later in range(phase + 1, phases):
                w_copy(array, split, later, got).start()

    def z_event(array, way, step):
        @pl.when(arrives(way, step))
        def _():
            z_copy(array, way, step).wait_recv()
            c_copy(array, way, step).start()

        if step + 1 < depth - 1:

            @pl.when(sends(way, step + 1))
            def _():
                z_copy(array, way, step + 1).start()

    w_events = [
        functools.partial(w_event, array, phase, index)
        for phase in range(phases)
        for index in range(1 << phase)
        for array in range(3)
    ]
    z_events = [
        [functools.partial(z_event, array, way, step) for way in range(2)]
        for step in range(depth - 1)
        for array in range(2)
    ]
    for i in range(max(len(w_events), len(z_events))):
        if i < len(w_events):
            w_events[i]()
        if i < len(z_events):
            for event in z_events[i]:
                event()

    for copy in local:
        copy.wait()
    for array in range(2):
        c_copy(array, 0, -1).wait_send()
        c_copy(array, 0, -1).wait_recv()
        for way in range(2):
            for step in range(depth - 1):

                @pl.when(sends(way, step))
                def _():
                    z_copy(array, way, step).wait_send()

                @pl.when(arrives(way, step))
                def _():
                    c_copy(array, way, step).wait_send()
                    c_copy(array, way, step).wait_recv()

    for array in range(3):
        for split in range(2):
            order = orders[split]
            for phase in range(phases):
                for index in range(1 << phase):
                    mask = sum(order[i] for i in range(phase) if index & (1 << i))
                    w_copy(array, split, phase, mask).wait_send()


def gather_all(n_fs, n_tp, *ins):
    tokens, gate, up, down, cot = ins
    depth = n_tp // CORES
    any_spec = pl.BlockSpec(memory_space=pl.ANY)
    vmem = pl.BlockSpec(memory_space=pltpu.VMEM)
    full = lambda a, axis, n: jax.ShapeDtypeStruct(
        tuple(s * n if i == axis else s for i, s in enumerate(a.shape)), a.dtype
    )
    dma = pltpu.SemaphoreType.DMA
    return pl.pallas_call(
        functools.partial(gather_kernel, n_fs, n_tp),
        out_shape=(
            full(tokens, 0, n_tp),
            full(gate, 1, n_fs),
            full(up, 1, n_fs),
            full(down, 1, n_fs),
            full(cot, 0, n_tp),
        ),
        in_specs=[vmem] * 5,
        out_specs=[any_spec] * 5,
        scratch_shapes=[
            dma((3, 2, n_fs - 1)),
            dma((3, 2, n_fs - 1)),
            dma((2, 2, max(depth - 1, 1))),
            dma((2, 2, max(depth - 1, 1))),
            dma((2, 2, depth)),
            dma((2, 2, depth)),
            dma((8,)),
        ],
        compiler_params=pltpu.CompilerParams(collective_id=0, has_side_effects=True),
        name="gather",
    )(*ins)


def scatter_kernel(n_fs, n_tp, *refs):
    gi_ref, *w_refs = refs[:4]
    gi_out, *w_outs = refs[4:8]
    stages, recvs = refs[8:11], refs[11:14]
    c_buf, z_stage, z_buf = refs[14:17]
    w_send, w_recv, z_send, z_recv, c_send, c_recv = refs[17:]
    fs, tp = lax.axis_index("fs"), lax.axis_index("tp")
    depth = n_tp // CORES
    z, core = tp // CORES, tp % CORES
    orders = orders_of(n_fs)
    phases = len(orders[0])
    f32 = jnp.float32
    greet(n_fs, depth, fs, tp, z)

    def w_own(array, split, mask):
        out = w_outs[array]
        half, cols = out.shape[0] // 2, out.shape[1]
        owner = fs ^ mask
        return w_refs[array].at[
            pl.ds(split * half, half), pl.ds(pl.multiple_of(owner * cols, cols), cols)
        ]

    def compact(order, mask):
        return sum(1 << i for i, bit in enumerate(order) if mask & bit)

    def w_copy(array, split, mask):
        order = orders[split]
        phase = first_bit(order, mask)
        slot = compact(order, mask) - 1
        src = w_own(array, split, mask) if phase == 0 else stages[array].at[split, slot]
        return pltpu.make_async_remote_copy(
            src_ref=src,
            dst_ref=recvs[array].at[split, slot],
            send_sem=w_send.at[array, split, slot],
            recv_sem=w_recv.at[array, split, slot],
            device_id=(fs ^ order[phase], tp),
            device_id_type=MESH,
        )

    def w_sum(array, split, mask):
        order = orders[split]
        total = w_own(array, split, mask)[...].astype(f32)
        limit = phases if mask == 0 else first_bit(order, mask)
        for phase in range(limit):
            sent = mask | order[phase]
            w_copy(array, split, sent).wait_recv()
            total += recvs[array][split, compact(order, sent) - 1].astype(f32)
        return total

    n = gi_out.shape[0]

    def g_rows(target, which):
        return pl.ds(pl.multiple_of((target * CORES + which) * n, n), n)

    def c_copy(target):
        return pltpu.make_async_remote_copy(
            src_ref=gi_ref.at[g_rows(target, 1 - core), :],
            dst_ref=c_buf.at[target],
            send_sem=c_send.at[target],
            recv_sem=c_recv.at[target],
            device_id=(fs, tp ^ 1),
            device_id_type=MESH,
        )

    def z_target(way, step):
        return depth - 1 - step if way == 0 else step

    def z_copy(way, step):
        return pltpu.make_async_remote_copy(
            src_ref=z_stage.at[way, step],
            dst_ref=z_buf.at[way, step],
            send_sem=z_send.at[way, step],
            recv_sem=z_recv.at[way, step],
            device_id=(fs, tp + CORES if way == 0 else tp - CORES),
            device_id_type=MESH,
        )

    def sends(way, step):
        t = z_target(way, step)
        return t > z if way == 0 else t < z

    def arrives(way, step):
        t = z_target(way, step)
        return jnp.logical_and(z > 0, t >= z) if way == 0 else jnp.logical_and(z < depth - 1, t <= z)

    targets = []
    for i in range(depth):
        t = depth - 1 - i // 2 if i % 2 == 0 else i // 2
        targets.append(t)
    for t in targets:
        c_copy(t).start()

    for array in range(3):
        for split in range(2):
            order = orders[split]
            masks = [m for m in range(1, n_fs) if m & order[0]]
            for mask in sorted(masks, key=lambda m: -compact(order, m)):
                w_copy(array, split, mask).start()

    both = c_buf
    for t in targets:
        c_copy(t).wait_recv()
        both[t] = (
            both[t].astype(f32) + gi_ref[g_rows(t, core), :].astype(f32)
        ).astype(both.dtype)

    def z_event(way, step):
        t = z_target(way, step)

        @pl.when(arrives(way, step))
        def _():
            z_copy(way, step).wait_recv()

        @pl.when(sends(way, step))
        def _():
            @pl.when(arrives(way, step))
            def _():
                z_stage[way, step] = (
                    both[t].astype(f32) + z_buf[way, step].astype(f32)
                ).astype(z_stage.dtype)

            @pl.when(jnp.logical_not(arrives(way, step)))
            def _():
                z_stage[way, step] = both[t]

            z_copy(way, step).start()

    def w_event(array, mask):
        for split in range(2):
            order = orders[split]
            real = sum(bit for i, bit in enumerate(order) if mask & (1 << i))
            slot = mask - 1
            stages[array][split, slot] = w_sum(array, split, real).astype(stages[array].dtype)
            w_copy(array, split, real).start()

    def w_finish(array):
        half = w_outs[array].shape[0] // 2
        for split in range(2):
            w_outs[array][pl.ds(split * half, half), :] = w_sum(array, split, 0)

    later = [m for m in range(1, n_fs) if not m & 1]
    later = sorted(later, key=lambda m: ((m & -m), -m))
    w_events = [functools.partial(w_event, array, mask) for array in range(3) for mask in later]
    z_events = [
        functools.partial(z_event, way, step) for step in range(depth - 1) for way in range(2)
    ]
    for event in z_events + w_events:
        event()

    total = both[z].astype(f32)
    zero = jnp.zeros_like(total)
    from_left = z_buf[0, jnp.clip(depth - 1 - z, 0, depth - 2)].astype(f32)
    from_right = z_buf[1, jnp.clip(z, 0, depth - 2)].astype(f32)
    total += jnp.where(z > 0, from_left, zero)
    total += jnp.where(z < depth - 1, from_right, zero)
    gi_out[...] = total.astype(gi_out.dtype)

    for array in range(3):
        w_finish(array)

    for t in targets:
        c_copy(t).wait_send()
    for way in range(2):
        for step in range(depth - 1):

            @pl.when(sends(way, step))
            def _():
                z_copy(way, step).wait_send()

    for array in range(3):
        for split in range(2):
            for mask in range(1, n_fs):
                w_copy(array, split, mask).wait_send()


def scatter_all(n_fs, n_tp, gi, gg, gu, gd):
    depth = n_tp // CORES
    f32 = jnp.float32
    vmem = pl.BlockSpec(memory_space=pltpu.VMEM)
    dma = pltpu.SemaphoreType.DMA
    shapes = tuple((g.shape[0], g.shape[1] // n_fs) for g in (gg, gu, gd))
    n, width = gi.shape[0] // n_tp, gi.shape[1]
    slots = [pltpu.VMEM((2, n_fs - 1, s[0] // 2, s[1]), gi.dtype) for s in shapes]
    return pl.pallas_call(
        functools.partial(scatter_kernel, n_fs, n_tp),
        out_shape=(jax.ShapeDtypeStruct((n, width), gi.dtype),)
        + tuple(jax.ShapeDtypeStruct(s, f32) for s in shapes),
        in_specs=[vmem] * 4,
        out_specs=[vmem] * 4,
        scratch_shapes=slots
        + slots
        + [
            pltpu.VMEM((depth, n, width), gi.dtype),
            pltpu.VMEM((2, depth - 1, n, width), gi.dtype),
            pltpu.VMEM((2, depth - 1, n, width), gi.dtype),
            dma((3, 2, n_fs - 1)),
            dma((3, 2, n_fs - 1)),
            dma((2, depth - 1)),
            dma((2, depth - 1)),
            dma((depth,)),
            dma((depth,)),
        ],
        compiler_params=pltpu.CompilerParams(
            collective_id=1, has_side_effects=True, vmem_limit_bytes=60 * 1024 * 1024
        ),
        name="scatter",
    )(gi, gg, gu, gd)


def body(n_fs, n_tp, tokens, gate_weight, up_weight, down_weight, grad_out):
    bf16 = tokens.dtype
    tok_all, gate_full, up_full, down_full, cot_all = gather_all(
        n_fs, n_tp, tokens, gate_weight.T, up_weight.T, down_weight, grad_out
    )
    gate_pre = over_cols(tok_all, gate_full)
    up_pre = over_cols(tok_all, up_full)
    sig_gate = jax.nn.sigmoid(gate_pre)
    active = gate_pre * sig_gate
    hidden = (active * up_pre).astype(bf16)
    d_hidden = over_cols(cot_all, down_full)
    d_gate = (d_hidden * up_pre * sig_gate * (1.0 + gate_pre * (1.0 - sig_gate))).astype(bf16)
    d_up = (d_hidden * active).astype(bf16)
    dot = functools.partial(jnp.dot, preferred_element_type=jnp.float32)
    grad_input = (dot(d_gate, gate_full) + dot(d_up, up_full)).astype(bf16)
    grad_input, grad_gate, grad_up, grad_down = scatter_all(
        n_fs,
        n_tp,
        grad_input,
        over_rows(d_gate, tok_all, bf16),
        over_rows(d_up, tok_all, bf16),
        over_rows(hidden, cot_all, bf16),
    )
    return grad_input, grad_gate.T, grad_up.T, grad_down


def solution(mesh):
    in_specs = (
        P(("fs", "tp"), None),
        P("fs", "tp"),
        P("fs", "tp"),
        P("tp", "fs"),
        P(("fs", "tp"), None),
    )
    out_specs = (P(("fs", "tp"), None), P("fs", "tp"), P("fs", "tp"), P("tp", "fs"))
    return jax.shard_map(
        functools.partial(body, mesh.shape["fs"], mesh.shape["tp"]),
        mesh=mesh,
        in_specs=in_specs,
        out_specs=out_specs,
        check_vma=False,
    )
```

profile of v0, /device:TPU:8, one launch (start us, length us, event | category | flops | bytes accessed | tf_op | source)
XLA Modules:
  0.0 249.8 jit_solution(8169199555894832147)
XLA Ops:
  0.6 76.0 %gather.1 = (bf16[1024,2048]{1,0:T(8,128)(2,1)}, bf16[704,2048]{1,0:T(8,128)(2,1)}, bf16[704,2048]{1,0:T(8,128)(2,1)}, bf16[704,2048]{1,0:T(8,128)(2,1)}, bf16[1024,2048]{1,0:T(8,128)(2,1)}) custom-call(bf16[128,2048]{1,0:T(8,128)(2,1)} %refs_0_.1, bf16[704,512]{1,0:T(8,128)(2,1)} %bitcast.21, bf16[704,512]{1,0:T(8,128)(2,1)} %bitcast.22, ...), custom_call_target="tpu_custom_call" | custom-call | tf_op jit(solution)/shard_map/gather/pallas_call | solution.py:226
  76.6 0.0 copy-start.2
  76.6 0.0 copy-start.5
  76.6 6.0 %fusion.3 = f32[1024,704]{0,1:T(8,128)S(1)} fusion(bf16[1024,2048]{1,0:T(8,128)(2,1)} %get-tuple-element.15, bf16[704,2048]{1,0:T(8,128)(2,1)} %get-tuple-element.16), kind=kOutput, calls=%fused_computation.10 | convolution fusion | flops 2952790016 | bytes 9961472 | tf_op jit(solution)/shard_map/dot_general | solution.py:21
  82.7 0.0 copy-done.2
  82.7 0.0 copy-done.5
  82.7 0.0 copy-start.3
  82.7 0.0 copy-start.6
  82.7 3.2 %fusion.4 = f32[1024,704]{0,1:T(8,128)S(1)} fusion(bf16[1024,2048]{1,0:T(8,128)(2,1)S(1)} %copy-done.2, bf16[704,2048]{1,0:T(8,128)(2,1)S(1)} %copy-done.5), kind=kOutput, calls=%fused_computation.11 | convolution fusion | flops 2952790016 | bytes 9961472 | tf_op jit(solution)/shard_map/dot_general | solution.py:21
  85.9 0.0 copy-done.3
  85.9 0.0 copy-done.6
  85.9 4.0 %multiply_convert_fusion.1 = (bf16[1024,704]{0,1:T(8,128)(2,1)S(1)}, bf16[1024,704]{0,1:T(8,128)(2,1)S(1)}) fusion(f32[1024,704]{0,1:T(8,128)S(1)} %fusion.4, f32[1024,704]{0,1:T(8,128)S(1)} %fusion.3, bf16[1024,2048]{1,0:T(8,128)(2,1)S(1)} %copy-done.3, bf16[704,2048]{1,0:T(8,128)(2,1)S(1)} %copy-done.6), kind=kOutput, calls=%fused_computation.5 | convolution fusion | flops 2962161664 | bytes 15728640 | tf_op jit(solution)/shard_map/dot_general | solution.py:21
  89.9 4.7 %convolution_convert_fusion.refs_3_ = bf16[704,2048]{1,0:T(8,128)(2,1)} fusion(bf16[1024,2048]{1,0:T(8,128)(2,1)S(1)} %copy-done.3, f32[1024,704]{0,1:T(8,128)S(1)} %fusion.3, f32[1024,704]{0,1:T(8,128)S(1)} %fusion.4), kind=kOutput, calls=%fused_computation.1 | convolution fusion | flops 2958557184 | bytes 12845056 | tf_op jit(solution)/shard_map/dot_general | solution.py:15
  94.6 4.5 %convolution_convert_fusion.1.refs_2_ = bf16[704,2048]{1,0:T(8,128)(2,1)} fusion(bf16[1024,704]{0,1:T(8,128)(2,1)S(1)} %get-tuple-element.22, bf16[1024,2048]{1,0:T(8,128)(2,1)S(1)} %copy-done.2), kind=kOutput, calls=%fused_computation.2 | convolution fusion | flops 2954231808 | bytes 8519680 | tf_op jit(solution)/shard_map/dot_general | solution.py:15
  99.2 4.5 %convolution_convert_fusion.2.refs_1_ = bf16[704,2048]{1,0:T(8,128)(2,1)} fusion(bf16[1024,704]{0,1:T(8,128)(2,1)S(1)} %get-tuple-element.23, bf16[1024,2048]{1,0:T(8,128)(2,1)S(1)} %copy-done.2), kind=kOutput, calls=%fused_computation.3 | convolution fusion | flops 2954231808 | bytes 8519680 | tf_op jit(solution)/shard_map/dot_general | solution.py:15
  103.7 0.0 copy-start.4
  103.7 3.5 %fusion.5 = f32[1024,2048]{1,0:T(8,128)S(1)} fusion(bf16[1024,704]{0,1:T(8,128)(2,1)S(1)} %get-tuple-element.23, bf16[704,2048]{1,0:T(8,128)(2,1)S(1)} %copy-done.5), kind=kOutput, calls=%fused_computation.12 | convolution fusion | flops 2952790016 | bytes 12713984 | tf_op jit(solution)/shard_map/dot_general | solution.py:474
  107.2 0.0 copy-done.4
  107.2 5.4 %add_convert_fusion.refs_0_ = bf16[1024,2048]{1,0:T(8,128)(2,1)} fusion(f32[1024,2048]{1,0:T(8,128)S(1)} %fusion.5, bf16[1024,704]{0,1:T(8,128)(2,1)S(1)} %get-tuple-element.22, bf16[704,2048]{1,0:T(8,128)(2,1)S(1)} %copy-done.4), kind=kOutput, calls=%fused_computation | convolution fusion | flops 2956984320 | bytes 16908288 | tf_op jit(solution)/shard_map/dot_general | solution.py:474
  112.6 130.4 %scatter.1 = (bf16[128,2048]{1,0:T(8,128)(2,1)}, f32[704,512]{1,0:T(8,128)}, f32[704,512]{1,0:T(8,128)}, f32[704,512]{1,0:T(8,128)}) custom-call(bf16[1024,2048]{1,0:T(8,128)(2,1)} %add_convert_fusion.refs_0_, bf16[704,2048]{1,0:T(8,128)(2,1)} %convolution_convert_fusion.2.refs_1_, bf16[704,2048]{1,0:T(8,128)(2,1)} %convolution_convert_fusion.1.refs_2_, ...), custom_call_target="tpu_custom_call" | custom-call | tf_op jit(solution)/shard_map/scatter/pallas_call | solution.py:434
  243.0 0.0 copy-start.1
  243.0 2.0 copy.13
  245.0 0.0 copy-start
  245.0 2.7 %copy.14 = f32[512,704]{0,1:T(8,128)} copy(f32[512,704]{0,1:T(8,128)} %bitcast.20) | data formatting | bytes 2883584
  247.6 0.0 copy-done.1
  247.6 1.1 copy.15
  248.7 0.0 copy-done
  248.7 1.1 copy.16
Async XLA Ops:
  76.6 6.0 %copy-start.2 = (bf16[1024,2048]{1,0:T(8,128)(2,1)S(1)}, bf16[1024,2048]{1,0:T(8,128)(2,1)}, u32[]{:S(2)}) copy-start(bf16[1024,2048]{1,0:T(8,128)(2,1)} %get-tuple-element.15) | copy-start | bytes 12582916
  76.6 6.0 %copy-start.5 = (bf16[704,2048]{1,0:T(8,128)(2,1)S(1)}, bf16[704,2048]{1,0:T(8,128)(2,1)}, u32[]{:S(2)}) copy-start(bf16[704,2048]{1,0:T(8,128)(2,1)} %get-tuple-element.17) | copy-start | bytes 8650756
  82.7 3.2 %copy-start.3 = (bf16[1024,2048]{1,0:T(8,128)(2,1)S(1)}, bf16[1024,2048]{1,0:T(8,128)(2,1)}, u32[]{:S(2)}) copy-start(bf16[1024,2048]{1,0:T(8,128)(2,1)} %get-tuple-element.13) | copy-start | bytes 12582916
  82.7 3.2 %copy-start.6 = (bf16[704,2048]{1,0:T(8,128)(2,1)S(1)}, bf16[704,2048]{1,0:T(8,128)(2,1)}, u32[]{:S(2)}) copy-start(bf16[704,2048]{1,0:T(8,128)(2,1)} %get-tuple-element.14) | copy-start | bytes 8650756
  103.7 3.5 %copy-start.4 = (bf16[704,2048]{1,0:T(8,128)(2,1)S(1)}, bf16[704,2048]{1,0:T(8,128)(2,1)}, u32[]{:S(2)}) copy-start(bf16[704,2048]{1,0:T(8,128)(2,1)} %get-tuple-element.16) | copy-start | bytes 8650756
  243.0 4.7 %copy-start.1 = (f32[704,512]{1,0:T(8,128)S(1)}, f32[704,512]{1,0:T(8,128)}, u32[]{:S(2)}) copy-start(f32[704,512]{1,0:T(8,128)} %get-tuple-element.20) | copy-start | bytes 4325380
  245.0 3.8 %copy-start = (f32[704,512]{1,0:T(8,128)S(1)}, f32[704,512]{1,0:T(8,128)}, u32[]{:S(2)}) copy-start(f32[704,512]{1,0:T(8,128)} %get-tuple-element.31) | copy-start | bytes 4325380
where the time goes:
time: 250 us
  Pallas kernels  206 us (82%)
  matrix products  35.8 us (14%)
  local copies, waits for them, and re-layouts  6.9 us (3%)
    pallas_call x1, Pallas kernels, scatter_all(): pl.pallas_call(functools.partial(scatter_kernel, n_fs, n_tp), out_shape=(...  130 us
    pallas_call x1, Pallas kernels, gather_all(): pl.pallas_call(functools.partial(gather_kernel, n_fs, n_tp), out_shape=(f...  76 us
    dot_general x3, matrix products, over_rows(): lax.dot_general(left, right, (((0,), (0,)), ((), ())), preferred_element_...  13.7 us
    dot_general x3, matrix products, over_cols(): lax.dot_general(left, right, (((1,), (1,)), ((), ())), preferred_element_...  13.2 us
    dot_general x2, matrix products, body(): grad_input = (dot(d_gate, gate_full) + dot(d_up, up_full)).astype(bf16)  8.88 us
    unnamed x18, local copies, waits for them, and re-layouts  6.9 us

commit v1 on v0

v1 whole, which is shorter than its diff:
```python
import functools

import jax
import jax.numpy as jnp
from jax import lax
from jax.experimental import pallas as pl
from jax.experimental.pallas import tpu as pltpu
from jax.sharding import PartitionSpec as P

MESH = pl.DeviceIdType.MESH
CORES = 2
PARTS = 2
F32 = jnp.float32


def nt(left, right):
    return lax.dot_general(left, right, (((1,), (1,)), ((), ())), preferred_element_type=F32)


def nn(left, right):
    return jnp.dot(left, right, preferred_element_type=F32)


def orders_of(n_fs):
    bits = [1 << i for i in range(n_fs.bit_length() - 1)]
    return (bits, bits[::-1])


def first_bit(order, mask):
    return next(i for i, bit in enumerate(order) if mask & bit)


def compact(order, mask):
    return sum(1 << i for i, bit in enumerate(order) if mask & bit)


def greet(n_fs, depth, fs, tp, z):
    barrier = pltpu.get_barrier_semaphore()
    bits = orders_of(n_fs)[0]

    def hello(fs_id, tp_id):
        pl.semaphore_signal(barrier, inc=1, device_id=(fs_id, tp_id), device_id_type=MESH)

    for bit in bits:
        hello(fs ^ bit, tp)
    hello(fs, tp ^ 1)

    @pl.when(z > 0)
    def _():
        hello(fs, tp - CORES)

    @pl.when(z < depth - 1)
    def _():
        hello(fs, tp + CORES)

    ends = (z > 0).astype(jnp.int32) + (z < depth - 1).astype(jnp.int32)
    pl.semaphore_wait(barrier, len(bits) + 1 + ends)


def layer_kernel(n_fs, n_tp, *refs):
    ins, outs, scratch = refs[:5], refs[5:9], refs[9:]
    tok_all, cot_all, gate_full, up_full, down_full = scratch[:5]
    act_buf, fac_buf, hid_t, dgate_t, dup_t, dgate, dup = scratch[5:12]
    grads, recvs, stages, w_res = scratch[12:15], scratch[15:18], scratch[18:21], scratch[21:24]
    gi, c_buf, z_buf, gi_res = scratch[24:28]
    gw_send, gw_recv, gz_send, gz_recv, gc_send, gc_recv, l_sem = scratch[28:35]
    sw_send, sw_recv, sz_send, sz_recv, sc_send, sc_recv, o_sem = scratch[35:]
    fs, tp = lax.axis_index("fs"), lax.axis_index("tp")
    depth = n_tp // CORES
    z, core = tp // CORES, tp % CORES
    orders = orders_of(n_fs)
    phases = len(orders[0])
    bf16 = tok_all.dtype
    rows_all, width = tok_all.shape
    n = rows_all // n_tp
    ff = gate_full.shape[0]
    cols = width // n_fs
    half = ff // 2
    sub = n // PARTS
    rows = (tok_all, cot_all)
    weights = (gate_full, up_full, down_full)

    def slab(owner):
        return pl.ds(pl.multiple_of(owner * cols, cols), cols)

    def own_rows(owner):
        return pl.ds(pl.multiple_of(owner * n, n), n)

    local = [
        pltpu.make_async_copy(ins[0], tok_all.at[own_rows(tp), :], l_sem.at[0]),
        pltpu.make_async_copy(ins[1], gate_full.at[:, slab(fs)], l_sem.at[1]),
        pltpu.make_async_copy(ins[2], up_full.at[:, slab(fs)], l_sem.at[2]),
        pltpu.make_async_copy(ins[3], down_full.at[:, slab(fs)], l_sem.at[3]),
        pltpu.make_async_copy(ins[4], cot_all.at[own_rows(tp), :], l_sem.at[4]),
    ]
    for copy in local:
        copy.start()
    greet(n_fs, depth, fs, tp, z)
    for copy in local:
        copy.wait()

    def gw_copy(array, split, phase, mask):
        order = orders[split]
        there = weights[array].at[pl.ds(split * half, half), slab(fs ^ mask)]
        slot = (array, split, (1 << phase) - 1 + sum(1 << i for i in range(phase) if mask & order[i]))
        return pltpu.make_async_remote_copy(
            src_ref=there,
            dst_ref=there,
            send_sem=gw_send.at[slot],
            recv_sem=gw_recv.at[slot],
            device_id=(fs ^ order[phase], tp),
            device_id_type=MESH,
        )

    def gw_start(array):
        for phase in range(phases):
            for split in range(2):
                gw_copy(array, split, phase, 0).start()

    def gw_event(array, phase, index):
        for split in range(2):
            order = orders[split]
            mask = sum(order[i] for i in range(phase) if index & (1 << i))
            gw_copy(array, split, phase, mask).wait_recv()
            got = mask | order[phase]
            for later in range(phase + 1, phases):
                gw_copy(array, split, later, got).start()

    def gw_relays(array):
        for phase in range(phases - 1):
            for index in range(1 << phase):
                gw_event(array, phase, index)

    def gw_finish(array):
        for index in range(1 << (phases - 1)):
            gw_event(array, phases - 1, index)

    def r_block(array, owner, part):
        start = pl.multiple_of(owner * n + part * sub, sub)
        return rows[array].at[pl.ds(start, sub), :]

    def gz_copy(array, way, step, part):
        sign = 1 if way == 0 else -1
        there = r_block(array, tp - sign * step * CORES, part)
        slot = (array, way, step, part)
        return pltpu.make_async_remote_copy(
            src_ref=there,
            dst_ref=there,
            send_sem=gz_send.at[slot],
            recv_sem=gz_recv.at[slot],
            device_id=(fs, tp + sign * CORES),
            device_id_type=MESH,
        )

    def g_sends(way, step):
        if way == 0:
            return jnp.logical_and(z - step >= 0, z < depth - 1)
        return jnp.logical_and(z + step <= depth - 1, z > 0)

    def g_arrives(way, step):
        return z - 1 - step >= 0 if way == 0 else z + 1 + step <= depth - 1

    def gc_copy(array, way, step, part):
        sign = 1 if way == 0 else -1
        there = r_block(array, tp - sign * (step + 1) * CORES, part)
        slot = (array, way, step + 1, part)
        return pltpu.make_async_remote_copy(
            src_ref=there,
            dst_ref=there,
            send_sem=gc_send.at[slot],
            recv_sem=gc_recv.at[slot],
            device_id=(fs, tp ^ 1),
            device_id_type=MESH,
        )

    def gz_start(array):
        for part in range(PARTS):
            for way in range(2):

                @pl.when(g_sends(way, 0))
                def _():
                    gz_copy(array, way, 0, part).start()

            gc_copy(array, 0, -1, part).start()

    def gz_event(array, step, part):
        for way in range(2):

            @pl.when(g_arrives(way, step))
            def _():
                gz_copy(array, way, step, part).wait_recv()

            if step + 1 < depth - 1:

                @pl.when(g_sends(way, step + 1))
                def _():
                    gz_copy(array, way, step + 1, part).start()

            @pl.when(g_arrives(way, step))
            def _():
                gc_copy(array, way, step, part).start()

    def gz_events(array, first, last):
        for step in range(first, last):
            for part in range(PARTS):
                gz_event(array, step, part)

    def gc_finish(array):
        for part in range(PARTS):
            gc_copy(array, 0, -1, part).wait_recv()
            for way in range(2):
                for step in range(depth - 1):

                    @pl.when(g_arrives(way, step))
                    def _():
                        gc_copy(array, way, step, part).wait_recv()

    def sw_own(array, split, mask):
        return grads[array].at[pl.ds(split * half, half), slab(fs ^ mask)]

    def sw_copy(array, split, mask):
        order = orders[split]
        phase = first_bit(order, mask)
        slot = compact(order, mask) - 1
        src = sw_own(array, split, mask) if phase == 0 else stages[array].at[split, slot // 2]
        return pltpu.make_async_remote_copy(
            src_ref=src,
            dst_ref=recvs[array].at[split, slot],
            send_sem=sw_send.at[array, split, slot],
            recv_sem=sw_recv.at[array, split, slot],
            device_id=(fs ^ order[phase], tp),
            device_id_type=MESH,
        )

    def sw_sum(array, split, mask):
        order = orders[split]
        total = sw_own(array, split, mask)[...].astype(F32)
        limit = phases if mask == 0 else first_bit(order, mask)
        for phase in range(limit):
            sent = mask | order[phase]
            sw_copy(array, split, sent).wait_recv()
            total += recvs[array][split, compact(order, sent) - 1].astype(F32)
        return total

    later = [m for m in range(1, n_fs) if not m & 1]
    later = sorted(later, key=lambda m: ((m & -m), -m))

    def sw_relay(array):
        for mask in later:
            for split in range(2):
                order = orders[split]
                real = sum(bit for i, bit in enumerate(order) if mask & (1 << i))
                slot = mask - 1
                stages[array][split, slot // 2] = sw_sum(array, split, real).astype(bf16)
                sw_copy(array, split, real).start()

    def sw_finish(array):
        for split in range(2):
            w_res[array][pl.ds(split * half, half), :] = sw_sum(array, split, 0)
        pltpu.make_async_copy(w_res[array], outs[1 + array], o_sem.at[1 + array]).start()

    firsts = (orders[0][0], orders[1][0])
    masks = sorted(
        range(n_fs), key=lambda m: (-sum(1 for b in firsts if m & b), -m)
    )

    def weight_grad(array, left, right):
        for mask in masks:
            grads[array][:, slab(fs ^ mask)] = nn(left[...], right[:, slab(fs ^ mask)]).astype(bf16)
            for split in range(2):
                if mask & firsts[split]:
                    sw_copy(array, split, mask).start()

    def g_rows(target, which, part):
        start = (target * CORES + which) * n + part * sub
        return pl.ds(pl.multiple_of(start, sub), sub)

    def sc_copy(target, part):
        return pltpu.make_async_remote_copy(
            src_ref=gi.at[g_rows(target, 1 - core, part), :],
            dst_ref=c_buf.at[target, part],
            send_sem=sc_send.at[target, part],
            recv_sem=sc_recv.at[target, part],
            device_id=(fs, tp ^ 1),
            device_id_type=MESH,
        )

    def z_target(way, step):
        return depth - 1 - step if way == 0 else step

    def sz_copy(way, step, part):
        return pltpu.make_async_remote_copy(
            src_ref=c_buf.at[z_target(way, step), part],
            dst_ref=z_buf.at[way, step, part],
            send_sem=sz_send.at[way, step, part],
            recv_sem=sz_recv.at[way, step, part],
            device_id=(fs, tp + CORES if way == 0 else tp - CORES),
            device_id_type=MESH,
        )

    def s_sends(way, step):
        t = z_target(way, step)
        return t > z if way == 0 else t < z

    def s_arrives(way, step):
        t = z_target(way, step)
        return jnp.logical_and(z > 0, t >= z) if way == 0 else jnp.logical_and(z < depth - 1, t <= z)

    targets = [depth - 1 - i // 2 if i % 2 == 0 else i // 2 for i in range(depth)]

    def sc_event(t):
        for part in range(PARTS):
            sc_copy(t, part).wait_recv()
            c_buf[t, part] = (
                c_buf[t, part].astype(F32) + gi[g_rows(t, core, part), :].astype(F32)
            ).astype(bf16)

    def sz_event(step):
        for part in range(PARTS):
            for way in range(2):
                t = z_target(way, step)

                @pl.when(s_arrives(way, step))
                def _():
                    sz_copy(way, step, part).wait_recv()

                @pl.when(s_sends(way, step))
                def _():
                    @pl.when(s_arrives(way, step))
                    def _():
                        c_buf[t, part] = (
                            c_buf[t, part].astype(F32) + z_buf[way, step, part].astype(F32)
                        ).astype(bf16)

                    sz_copy(way, step, part).start()

    def sz_finish():
        zero = jnp.zeros((sub, width), F32)
        for part in range(PARTS):
            total = c_buf[z, part].astype(F32)
            from_left = z_buf[0, jnp.clip(depth - 1 - z, 0, depth - 2), part].astype(F32)
            from_right = z_buf[1, jnp.clip(z, 0, depth - 2), part].astype(F32)
            total += jnp.where(z > 0, from_left, zero)
            total += jnp.where(z < depth - 1, from_right, zero)
            gi_res[pl.ds(part * sub, sub), :] = total.astype(bf16)
        pltpu.make_async_copy(gi_res, outs[0], o_sem.at[0]).start()

    tile = min(256, rows_all)

    def over_tiles(step):
        def run(i, carry):
            step(pl.ds(pl.multiple_of(i * tile, tile), tile))
            return carry

        lax.fori_loop(0, rows_all // tile, run, 0)

    def gate_step(at):
        act_buf[:, at] = nt(gate_full[...], tok_all[at, :])

    def up_step(at):
        up_pre = nt(up_full[...], tok_all[at, :])
        gate_pre = act_buf[:, at]
        sig = jax.nn.sigmoid(gate_pre)
        active = gate_pre * sig
        hid_t[:, at] = (active * up_pre).astype(bf16)
        act_buf[:, at] = active
        fac_buf[:, at] = up_pre * sig * (1.0 + gate_pre * (1.0 - sig))

    def down_step(at):
        d_hidden = nt(down_full[...], cot_all[at, :])
        d_gate = d_hidden * fac_buf[:, at]
        d_up = d_hidden * act_buf[:, at]
        dgate_t[:, at] = d_gate.astype(bf16)
        dup_t[:, at] = d_up.astype(bf16)
        dgate[at, :] = d_gate.T.astype(bf16)
        dup[at, :] = d_up.T.astype(bf16)

    gi_tile = min(512, width)

    def gi_steps(first, last):
        def run(i, carry):
            at = pl.ds(pl.multiple_of(i * gi_tile, gi_tile), gi_tile)
            gi[:, at] = (nn(dgate[...], gate_full[:, at]) + nn(dup[...], up_full[:, at])).astype(bf16)
            return carry

        lax.fori_loop(first, last, run, 0)

    TOK, COT = 0, 1
    GATE, UP, DOWN = 0, 1, 2

    gz_start(TOK)
    gw_start(GATE)
    gz_event(TOK, 0, 0)
    gw_relays(GATE)
    gw_start(UP)
    for part in range(1, PARTS):
        gz_event(TOK, 0, part)
    gz_events(TOK, 1, depth - 2)
    gz_start(COT)
    gw_finish(GATE)
    gz_event(TOK, depth - 2, 0)
    gw_relays(UP)
    gw_start(DOWN)
    for part in range(1, PARTS):
        gz_event(TOK, depth - 2, part)
    gc_finish(TOK)
    over_tiles(gate_step)
    gz_events(COT, 0, 1)
    gw_finish(UP)
    over_tiles(up_step)
    gz_events(COT, 1, depth - 2)
    gw_relays(DOWN)
    gz_events(COT, depth - 2, depth - 1)
    gc_finish(COT)
    weight_grad(2, hid_t, cot_all)
    gw_finish(DOWN)
    over_tiles(down_step)
    gi_count = width // gi_tile
    gi_steps(0, gi_count // 2)
    sw_relay(2)
    gi_steps(gi_count // 2, gi_count)
    for t in targets:
        for part in range(PARTS):
            sc_copy(t, part).start()
    weight_grad(0, dgate_t, tok_all)
    for t in targets:
        sc_event(t)
    sz_event(0)
    weight_grad(1, dup_t, tok_all)
    for step in range(1, depth - 2):
        sz_event(step)
    sw_relay(0)
    sw_finish(2)
    for step in range(max(depth - 2, 1), depth - 1):
        sz_event(step)
    sw_relay(1)
    sz_finish()
    sw_finish(0)
    sw_finish(1)

    for array in range(2):
        for part in range(PARTS):
            gc_copy(array, 0, -1, part).wait_send()
            for way in range(2):
                for step in range(depth - 1):

                    @pl.when(g_sends(way, step))
                    def _():
                        gz_copy(array, way, step, part).wait_send()

                    @pl.when(g_arrives(way, step))
                    def _():
                        gc_copy(array, way, step, part).wait_send()

    for array in range(3):
        for split in range(2):
            order = orders[split]
            for phase in range(phases):
                for index in range(1 << phase):
                    mask = sum(order[i] for i in range(phase) if index & (1 << i))
                    gw_copy(array, split, phase, mask).wait_send()
            for mask in range(1, n_fs):
                sw_copy(array, split, mask).wait_send()

    for part in range(PARTS):
        for t in targets:
            sc_copy(t, part).wait_send()
        for way in range(2):
            for step in range(depth - 1):

                @pl.when(s_sends(way, step))
                def _():
                    sz_copy(way, step, part).wait_send()

    pltpu.make_async_copy(gi_res, outs[0], o_sem.at[0]).wait()
    for array in range(3):
        pltpu.make_async_copy(w_res[array], outs[1 + array], o_sem.at[1 + array]).wait()


def layer(n_fs, n_tp, tokens, gate, up, down, cot):
    depth = n_tp // CORES
    n, width = tokens.shape
    ff, cols = gate.shape
    rows_all = n * n_tp
    bf16 = tokens.dtype
    hbm = pl.BlockSpec(memory_space=pl.ANY)
    vmem = pltpu.VMEM
    dma = pltpu.SemaphoreType.DMA
    half, sub = ff // 2, n // PARTS
    n_stage = max(n_fs // 2 - 1, 1)
    scratch = (
        [vmem((rows_all, width), bf16)] * 2
        + [vmem((ff, width), bf16)] * 3
        + [vmem((ff, rows_all), F32)] * 2
        + [vmem((ff, rows_all), bf16)] * 3
        + [vmem((rows_all, ff), bf16)] * 2
        + [vmem((ff, width), bf16)] * 3
        + [vmem((2, n_fs - 1, half, cols), bf16)] * 3
        + [vmem((2, n_stage, half, cols), bf16)] * 3
        + [vmem((ff, cols), F32)] * 3
        + [
            vmem((rows_all, width), bf16),
            vmem((depth, PARTS, sub, width), bf16),
            vmem((2, depth - 1, PARTS, sub, width), bf16),
            vmem((n, width), bf16),
        ]
        + [
            dma((3, 2, n_fs - 1)),
            dma((3, 2, n_fs - 1)),
            dma((2, 2, depth - 1, PARTS)),
            dma((2, 2, depth - 1, PARTS)),
            dma((2, 2, depth, PARTS)),
            dma((2, 2, depth, PARTS)),
            dma((5,)),
            dma((3, 2, n_fs - 1)),
            dma((3, 2, n_fs - 1)),
            dma((2, depth - 1, PARTS)),
            dma((2, depth - 1, PARTS)),
            dma((depth, PARTS)),
            dma((depth, PARTS)),
            dma((4,)),
        ]
    )
    return pl.pallas_call(
        functools.partial(layer_kernel, n_fs, n_tp),
        out_shape=(jax.ShapeDtypeStruct((n, width), bf16),)
        + tuple(jax.ShapeDtypeStruct((ff, cols), F32) for _ in range(3)),
        in_specs=[hbm] * 5,
        out_specs=[hbm] * 4,
        scratch_shapes=scratch,
        compiler_params=pltpu.CompilerParams(
            collective_id=0, has_side_effects=True, vmem_limit_bytes=67043328
        ),
        name="layer",
    )(tokens, gate, up, down, cot)


def body(n_fs, n_tp, tokens, gate_weight, up_weight, down_weight, grad_out):
    grad_input, grad_gate, grad_up, grad_down = layer(
        n_fs, n_tp, tokens, gate_weight.T, up_weight.T, down_weight, grad_out
    )
    return grad_input, grad_gate.T, grad_up.T, grad_down


def solution(mesh):
    in_specs = (
        P(("fs", "tp"), None),
        P("fs", "tp"),
        P("fs", "tp"),
        P("tp", "fs"),
        P(("fs", "tp"), None),
    )
    out_specs = (P(("fs", "tp"), None), P("fs", "tp"), P("fs", "tp"), P("tp", "fs"))
    return jax.shard_map(
        functools.partial(body, mesh.shape["fs"], mesh.shape["tp"]),
        mesh=mesh,
        in_specs=in_specs,
        out_specs=out_specs,
        check_vma=False,
    )
```

time: 250 us -> 220 us (0.88)
  the two profiles are of different devices: /device:TPU:8 before, /device:TPU:10 now
where the time goes in v1:
time: 220 us
  Pallas kernels  212 us (96%)
  local copies, waits for them, and re-layouts  7.54 us (3%)
    pallas_call x1, Pallas kernels, layer(): pl.pallas_call(functools.partial(layer_kernel, n_fs, n_tp), out_shape=(ja...  212 us
    unnamed x8, local copies, waits for them, and re-layouts  7.54 us

profile of v1, /device:TPU:10, one launch (start us, length us, event | category | flops | bytes accessed | tf_op | source)
XLA Modules:
  0.0 219.8 jit_solution(11224401509130932603)
XLA Ops:
  0.6 211.6 %layer.1 = (bf16[128,2048]{1,0:T(8,128)(2,1)}, f32[704,512]{1,0:T(8,128)}, f32[704,512]{1,0:T(8,128)}, f32[704,512]{1,0:T(8,128)}) custom-call(bf16[128,2048]{1,0:T(8,128)(2,1)} %refs_0_.1, bf16[704,512]{1,0:T(8,128)(2,1)} %bitcast.6, bf16[704,512]{1,0:T(8,128)(2,1)} %bitcast.7, bf16[704,512]{1,0:T(8,128)(2,1)} %refs_3_.1, bf16[128,2048]{1,0:T(8,128)(2,1)} %refs_4_.1), custom_call_target="tpu_custom_call" | custom-call | tf_op jit(solution)/shard_map/layer/pallas_call | solution.py:524
  212.3 1.9 copy.13
  214.1 0.0 copy-start.1
  214.1 2.7 %copy.14 = f32[512,704]{0,1:T(8,128)} copy(f32[512,704]{0,1:T(8,128)} %bitcast.5) | data formatting | bytes 2883584
  216.8 0.0 copy-done.1
  216.8 0.0 copy-start
  216.8 1.1 copy.15
  217.9 0.8 copy-done
  218.7 1.1 copy.16
Async XLA Ops:
  214.1 2.7 %copy-start.1 = (f32[704,512]{1,0:T(8,128)S(1)}, f32[704,512]{1,0:T(8,128)}, u32[]{:S(2)}) copy-start(f32[704,512]{1,0:T(8,128)} %get-tuple-element.10) | copy-start | bytes 4325380
  216.8 1.9 copy-start

commit v2 on v1

--- a/solution.py
+++ b/solution.py
@@ -285,12 +285,15 @@
             device_id_type=MESH,
         )
 
-    def z_target(way, step):
+    def sz_from(way):
+        return z if way == 0 else depth - 1 - z
+
+    def sz_target(way, step):
         return depth - 1 - step if way == 0 else step
 
     def sz_copy(way, step, part):
         return pltpu.make_async_remote_copy(
-            src_ref=c_buf.at[z_target(way, step), part],
+            src_ref=c_buf.at[sz_target(way, step), part],
             dst_ref=z_buf.at[way, step, part],
             send_sem=sz_send.at[way, step, part],
             recv_sem=sz_recv.at[way, step, part],
@@ -299,12 +302,7 @@
         )
 
     def s_sends(way, step):
-        t = z_target(way, step)
-        return t > z if way == 0 else t < z
-
-    def s_arrives(way, step):
-        t = z_target(way, step)
-        return jnp.logical_and(z > 0, t >= z) if way == 0 else jnp.logical_and(z < depth - 1, t <= z)
+        return step < depth - 1 - sz_from(way)
 
     targets = [depth - 1 - i // 2 if i % 2 == 0 else i // 2 for i in range(depth)]
 
@@ -315,23 +313,29 @@
                 c_buf[t, part].astype(F32) + gi[g_rows(t, core, part), :].astype(F32)
             ).astype(bf16)
 
-    def sz_event(step):
-        for part in range(PARTS):
-            for way in range(2):
-                t = z_target(way, step)
-
-                @pl.when(s_arrives(way, step))
-                def _():
-                    sz_copy(way, step, part).wait_recv()
+    def sz_start():
+        for step in range(depth - 1):
+            for part in range(PARTS):
+                for way in range(2):
+
+                    @pl.when(sz_from(way) == 0)
+                    def _():
+                        sz_copy(way, step, part).start()
+
+    def sz_event(hop, part):
+        for way in range(2):
+            step = hop - sz_from(way)
+
+            @pl.when(jnp.logical_and(sz_from(way) > 0, step >= 0))
+            def _():
+                sz_copy(way, step, part).wait_recv()
 
                 @pl.when(s_sends(way, step))
                 def _():
-                    @pl.when(s_arrives(way, step))
-                    def _():
-                        c_buf[t, part] = (
-                            c_buf[t, part].astype(F32) + z_buf[way, step, part].astype(F32)
-                        ).astype(bf16)
-
+                    t = sz_target(way, step)
+                    c_buf[t, part] = (
+                        c_buf[t, part].astype(F32) + z_buf[way, step, part].astype(F32)
+                    ).astype(bf16)
                     sz_copy(way, step, part).start()
 
     def sz_finish():
@@ -425,15 +429,16 @@
     weight_grad(0, dgate_t, tok_all)
     for t in targets:
         sc_event(t)
-    sz_event(0)
+    sz_start()
     weight_grad(1, dup_t, tok_all)
-    for step in range(1, depth - 2):
-        sz_event(step)
-    sw_relay(0)
     sw_finish(2)
-    for step in range(max(depth - 2, 1), depth - 1):
-        sz_event(step)
-    sw_relay(1)
+    for hop in range(1, depth):
+        for part in range(PARTS):
+            sz_event(hop, part)
+        if hop == 1:
+            sw_relay(0)
+        if hop == max(depth - 2, 1):
+            sw_relay(1)
     sz_finish()
     sw_finish(0)
     sw_finish(1)

time: 220 us -> 158 us (0.72)
  the two profiles are of different devices: /device:TPU:10 before, /device:TPU:1 now
where the time goes in v2:
time: 158 us
  Pallas kernels  150 us (95%)
  local copies, waits for them, and re-layouts  7.54 us (5%)
    pallas_call x1, Pallas kernels, layer(): pl.pallas_call(functools.partial(layer_kernel, n_fs, n_tp), out_shape=(ja...  150 us
    unnamed x8, local copies, waits for them, and re-layouts  7.54 us

profile of v2, /device:TPU:1, one launch (start us, length us, event | category | flops | bytes accessed | tf_op | source)
XLA Modules:
  0.0 157.8 jit_solution(4858268338622509674)
XLA Ops:
  0.6 149.6 %layer.1 = (bf16[128,2048]{1,0:T(8,128)(2,1)}, f32[704,512]{1,0:T(8,128)}, f32[704,512]{1,0:T(8,128)}, f32[704,512]{1,0:T(8,128)}) custom-call(bf16[128,2048]{1,0:T(8,128)(2,1)} %refs_0_.1, bf16[704,512]{1,0:T(8,128)(2,1)} %bitcast.6, bf16[704,512]{1,0:T(8,128)(2,1)} %bitcast.7, bf16[704,512]{1,0:T(8,128)(2,1)} %refs_3_.1, bf16[128,2048]{1,0:T(8,128)(2,1)} %refs_4_.1), custom_call_target="tpu_custom_call" | custom-call | tf_op jit(solution)/shard_map/layer/pallas_call | solution.py:529
  150.2 1.9 %copy.13 = bf16[128,2048]{1,0:T(8,128)(2,1)} copy(bf16[128,2048]{1,0:T(8,128)(2,1)} %get-tuple-element.16) | data formatting | bytes 1048576
  152.1 0.0 copy-start.1
  152.1 2.7 %copy.14 = f32[512,704]{0,1:T(8,128)} copy(f32[512,704]{0,1:T(8,128)} %bitcast.5) | data formatting | bytes 2883584
  154.8 0.0 copy-done.1
  154.8 0.0 copy-start
  154.8 1.1 copy.15
  155.9 0.8 copy-done
  156.7 1.1 copy.16
Async XLA Ops:
  152.1 2.7 %copy-start.1 = (f32[704,512]{1,0:T(8,128)S(1)}, f32[704,512]{1,0:T(8,128)}, u32[]{:S(2)}) copy-start(f32[704,512]{1,0:T(8,128)} %get-tuple-element.10) | copy-start | bytes 4325380
  154.8 1.9 %copy-start = (f32[704,512]{1,0:T(8,128)S(1)}, f32[704,512]{1,0:T(8,128)}, u32[]{:S(2)}) copy-start(f32[704,512]{1,0:T(8,128)} %get-tuple-element.19) | copy-start | bytes 4325380

commit v3 on v2

--- a/solution.py
+++ b/solution.py
@@ -61,10 +61,10 @@
     ins, outs, scratch = refs[:5], refs[5:9], refs[9:]
     tok_all, cot_all, gate_full, up_full, down_full = scratch[:5]
     act_buf, fac_buf, hid_t, dgate_t, dup_t, dgate, dup = scratch[5:12]
-    grads, recvs, stages, w_res = scratch[12:15], scratch[15:18], scratch[18:21], scratch[21:24]
-    gi, c_buf, z_buf, gi_res = scratch[24:28]
-    gw_send, gw_recv, gz_send, gz_recv, gc_send, gc_recv, l_sem = scratch[28:35]
-    sw_send, sw_recv, sz_send, sz_recv, sc_send, sc_recv, o_sem = scratch[35:]
+    grads, recvs, stages = scratch[12:15], scratch[15:18], scratch[18:21]
+    gi, c_buf, z_buf = scratch[21:24]
+    gw_send, gw_recv, gz_send, gz_recv, gc_send, gc_recv, l_sem = scratch[24:31]
+    sw_send, sw_recv, sz_send, sz_recv, sc_send, sc_recv = scratch[31:]
     fs, tp = lax.axis_index("fs"), lax.axis_index("tp")
     depth = n_tp // CORES
     z, core = tp // CORES, tp % CORES
@@ -79,6 +79,7 @@
     sub = n // PARTS
     rows = (tok_all, cot_all)
     weights = (gate_full, up_full, down_full)
+    gi_res, *w_res = outs
 
     def slab(owner):
         return pl.ds(pl.multiple_of(owner * cols, cols), cols)
@@ -257,7 +258,6 @@
     def sw_finish(array):
         for split in range(2):
             w_res[array][pl.ds(split * half, half), :] = sw_sum(array, split, 0)
-        pltpu.make_async_copy(w_res[array], outs[1 + array], o_sem.at[1 + array]).start()
 
     firsts = (orders[0][0], orders[1][0])
     masks = sorted(
@@ -347,7 +347,45 @@
             total += jnp.where(z > 0, from_left, zero)
             total += jnp.where(z < depth - 1, from_right, zero)
             gi_res[pl.ds(part * sub, sub), :] = total.astype(bf16)
-        pltpu.make_async_copy(gi_res, outs[0], o_sem.at[0]).start()
+
+    def g_drain():
+        for array in range(2):
+            for part in range(PARTS):
+                gc_copy(array, 0, -1, part).wait_send()
+                for way in range(2):
+                    for step in range(depth - 1):
+
+                        @pl.when(g_sends(way, step))
+                        def _():
+                            gz_copy(array, way, step, part).wait_send()
+
+                        @pl.when(g_arrives(way, step))
+                        def _():
+                            gc_copy(array, way, step, part).wait_send()
+
+        for array in range(3):
+            for split in range(2):
+                order = orders[split]
+                for phase in range(phases):
+                    for index in range(1 << phase):
+                        mask = sum(order[i] for i in range(phase) if index & (1 << i))
+                        gw_copy(array, split, phase, mask).wait_send()
+
+    def sz_drain():
+        for part in range(PARTS):
+            for t in targets:
+                sc_copy(t, part).wait_send()
+            for way in range(2):
+                for step in range(depth - 1):
+
+                    @pl.when(s_sends(way, step))
+                    def _():
+                        sz_copy(way, step, part).wait_send()
+
+    def sw_drain(array):
+        for split in range(2):
+            for mask in range(1, n_fs):
+                sw_copy(array, split, mask).wait_send()
 
     tile = min(256, rows_all)
 
@@ -431,7 +469,9 @@
         sc_event(t)
     sz_start()
     weight_grad(1, dup_t, tok_all)
+    g_drain()
     sw_finish(2)
+    sw_drain(2)
     for hop in range(1, depth):
         for part in range(PARTS):
             sz_event(hop, part)
@@ -440,46 +480,12 @@
         if hop == max(depth - 2, 1):
             sw_relay(1)
     sz_finish()
+    sz_drain()
     sw_finish(0)
     sw_finish(1)
 
-    for array in range(2):
-        for part in range(PARTS):
-            gc_copy(array, 0, -1, part).wait_send()
-            for way in range(2):
-                for step in range(depth - 1):
-
-                    @pl.when(g_sends(way, step))
-                    def _():
-                        gz_copy(array, way, step, part).wait_send()
-
-                    @pl.when(g_arrives(way, step))
-                    def _():
-                        gc_copy(array, way, step, part).wait_send()
-
-    for array in range(3):
-        for split in range(2):
-            order = orders[split]
-            for phase in range(phases):
-                for index in range(1 << phase):
-                    mask = sum(order[i] for i in range(phase) if index & (1 << i))
-                    gw_copy(array, split, phase, mask).wait_send()
-            for mask in range(1, n_fs):
-                sw_copy(array, split, mask).wait_send()
-
-    for part in range(PARTS):
-        for t in targets:
-            sc_copy(t, part).wait_send()
-        for way in range(2):
-            for step in range(depth - 1):
-
-                @pl.when(s_sends(way, step))
-                def _():
-                    sz_copy(way, step, part).wait_send()
-
-    pltpu.make_async_copy(gi_res, outs[0], o_sem.at[0]).wait()
-    for array in range(3):
-        pltpu.make_async_copy(w_res[array], outs[1 + array], o_sem.at[1 + array]).wait()
+    sw_drain(0)
+    sw_drain(1)
 
 
 def layer(n_fs, n_tp, tokens, gate, up, down, cot):
@@ -502,12 +508,10 @@
         + [vmem((ff, width), bf16)] * 3
         + [vmem((2, n_fs - 1, half, cols), bf16)] * 3
         + [vmem((2, n_stage, half, cols), bf16)] * 3
-        + [vmem((ff, cols), F32)] * 3
         + [
             vmem((rows_all, width), bf16),
             vmem((depth, PARTS, sub, width), bf16),
             vmem((2, depth - 1, PARTS, sub, width), bf16),
-            vmem((n, width), bf16),
         ]
         + [
             dma((3, 2, n_fs - 1)),
@@ -523,27 +527,45 @@
             dma((2, depth - 1, PARTS)),
             dma((depth, PARTS)),
             dma((depth, PARTS)),
-            dma((4,)),
         ]
     )
     return pl.pallas_call(
         functools.partial(layer_kernel, n_fs, n_tp),
-        out_shape=(jax.ShapeDtypeStruct((n, width), bf16),)
-        + tuple(jax.ShapeDtypeStruct((ff, cols), F32) for _ in range(3)),
+        out_shape=(vmem((n, width), bf16),) + (vmem((ff, cols), F32),) * 3,
         in_specs=[hbm] * 5,
-        out_specs=[hbm] * 4,
+        out_specs=[pl.BlockSpec(memory_space=vmem)] * 4,
         scratch_shapes=scratch,
         compiler_params=pltpu.CompilerParams(
-            collective_id=0, has_side_effects=True, vmem_limit_bytes=67043328
+            collective_id=0, has_side_effects=True, vmem_limit_bytes=61000000
         ),
         name="layer",
     )(tokens, gate, up, down, cot)
 
 
+def deliver_kernel(*refs):
+    ins, outs, sem = refs[:4], refs[4:8], refs[8]
+    copies = [pltpu.make_async_copy(a, b, sem.at[i]) for i, (a, b) in enumerate(zip(ins, outs))]
+    for copy in copies:
+        copy.start()
+    for copy in copies:
+        copy.wait()
+
+
+def deliver(*arrays):
+    return pl.pallas_call(
+        deliver_kernel,
+        out_shape=tuple(jax.ShapeDtypeStruct(a.shape, a.dtype) for a in arrays),
+        in_specs=[pl.BlockSpec(memory_space=pltpu.VMEM)] * 4,
+        out_specs=[pl.BlockSpec(memory_space=pl.ANY)] * 4,
+        scratch_shapes=[pltpu.SemaphoreType.DMA((4,))],
+        compiler_params=pltpu.CompilerParams(vmem_limit_bytes=1 << 20),
+        name="deliver",
+    )(*arrays)
+
+
 def body(n_fs, n_tp, tokens, gate_weight, up_weight, down_weight, grad_out):
-    grad_input, grad_gate, grad_up, grad_down = layer(
-        n_fs, n_tp, tokens, gate_weight.T, up_weight.T, down_weight, grad_out
-    )
+    results = layer(n_fs, n_tp, tokens, gate_weight.T, up_weight.T, down_weight, grad_out)
+    grad_input, grad_gate, grad_up, grad_down = deliver(*results)
     return grad_input, grad_gate.T, grad_up.T, grad_down
 
 

time: 158 us -> 152 us (0.962)
  local copies, waits for them, and re-layouts: 7.54 us -> 0 us
    unnamed x8 -> x0, local copies, waits for them, and re-layouts: 7.54 us -> none
    pallas_call x1 -> x2, Pallas kernels: 150 us -> 151 us  [the longest x1 148 us: layer(): pl.pallas_call(functools.partial(layer_kernel, n_fs, n_tp), out_shape=(vm...]
where the time goes in v3:
time: 152 us
  Pallas kernels  151 us (99%)
    pallas_call x1, Pallas kernels, layer(): pl.pallas_call(functools.partial(layer_kernel, n_fs, n_tp), out_shape=(vm...  148 us

profile of v3, /device:TPU:1, one launch (start us, length us, event | category | flops | bytes accessed | tf_op | source)
XLA Modules:
  0.0 151.5 jit_solution(17401725133353169458)
XLA Ops:
  0.6 148.5 %layer.1 = (bf16[128,2048]{1,0:T(8,128)(2,1)S(1)}, f32[704,512]{1,0:T(8,128)S(1)}, f32[704,512]{1,0:T(8,128)S(1)}, f32[704,512]{1,0:T(8,128)S(1)}) custom-call(bf16[128,2048]{1,0:T(8,128)(2,1)} %refs_0_.1, bf16[704,512]{1,0:T(8,128)(2,1)} %bitcast.4, bf16[704,512]{1,0:T(8,128)(2,1)} %bitcast.5, bf16[704,512]{1,0:T(8,128)(2,1)} %refs_3_.1, ...), custom_call_target="tpu_custom_call" | custom-call | tf_op jit(solution)/shard_map/layer/pallas_call | solution.py:532
  149.1 2.3 %deliver.1 = (bf16[128,2048]{1,0:T(8,128)(2,1)}, f32[704,512]{1,0:T(8,128)}, f32[704,512]{1,0:T(8,128)}, f32[704,512]{1,0:T(8,128)}) custom-call(bf16[128,2048]{1,0:T(8,128)(2,1)S(1)} %get-tuple-element.12.refs_0_, f32[704,512]{1,0:T(8,128)S(1)} %get-tuple-element.13.refs_1_, f32[704,512]{1,0:T(8,128)S(1)} %get-tuple-element.14.refs_2_, ...), custom_call_target="tpu_custom_call" | custom-call | tf_op jit(solution)/shard_map/deliver/pallas_call | solution.py:555

commit v4 on v3

--- a/solution.py
+++ b/solution.py
@@ -32,6 +32,10 @@
 
 def compact(order, mask):
     return sum(1 << i for i, bit in enumerate(order) if mask & bit)
+
+
+def wait_bytes(ref, sem):
+    pltpu.make_async_copy(ref, ref, sem).wait()
 
 
 def greet(n_fs, depth, fs, tp, z):
@@ -103,12 +107,12 @@
     def gw_copy(array, split, phase, mask):
         order = orders[split]
         there = weights[array].at[pl.ds(split * half, half), slab(fs ^ mask)]
-        slot = (array, split, (1 << phase) - 1 + sum(1 << i for i in range(phase) if mask & order[i]))
+        slot = (1 << phase) - 1 + sum(1 << i for i in range(phase) if mask & order[i])
         return pltpu.make_async_remote_copy(
             src_ref=there,
             dst_ref=there,
-            send_sem=gw_send.at[slot],
-            recv_sem=gw_recv.at[slot],
+            send_sem=gw_send.at[array],
+            recv_sem=gw_recv.at[array, split, min(slot, n_fs // 2 - 1)],
             device_id=(fs ^ order[phase], tp),
             device_id_type=MESH,
         )
@@ -133,8 +137,11 @@
                 gw_event(array, phase, index)
 
     def gw_finish(array):
-        for index in range(1 << (phases - 1)):
-            gw_event(array, phases - 1, index)
+        last = n_fs // 2
+        for split in range(2):
+            half_rows = pl.ds(split * half, half)
+            landed = weights[array].at[half_rows, pl.ds(0, last * cols)]
+            wait_bytes(landed, gw_recv.at[array, split, last - 1])
 
     def r_block(array, owner, part):
         start = pl.multiple_of(owner * n + part * sub, sub)
@@ -143,12 +150,11 @@
     def gz_copy(array, way, step, part):
         sign = 1 if way == 0 else -1
         there = r_block(array, tp - sign * step * CORES, part)
-        slot = (array, way, step, part)
         return pltpu.make_async_remote_copy(
             src_ref=there,
             dst_ref=there,
-            send_sem=gz_send.at[slot],
-            recv_sem=gz_recv.at[slot],
+            send_sem=gz_send.at[array, way, step],
+            recv_sem=gz_recv.at[array, way, step, part],
             device_id=(fs, tp + sign * CORES),
             device_id_type=MESH,
         )
@@ -164,12 +170,11 @@
     def gc_copy(array, way, step, part):
         sign = 1 if way == 0 else -1
         there = r_block(array, tp - sign * (step + 1) * CORES, part)
-        slot = (array, way, step + 1, part)
         return pltpu.make_async_remote_copy(
             src_ref=there,
             dst_ref=there,
-            send_sem=gc_send.at[slot],
-            recv_sem=gc_recv.at[slot],
+            send_sem=gc_send.at[array],
+            recv_sem=gc_recv.at[array],
             device_id=(fs, tp ^ 1),
             device_id_type=MESH,
         )
@@ -207,14 +212,7 @@
                 gz_event(array, step, part)
 
     def gc_finish(array):
-        for part in range(PARTS):
-            gc_copy(array, 0, -1, part).wait_recv()
-            for way in range(2):
-                for step in range(depth - 1):
-
-                    @pl.when(g_arrives(way, step))
-                    def _():
-                        gc_copy(array, way, step, part).wait_recv()
+        wait_bytes(rows[array].at[pl.ds(0, rows_all // CORES), :], gc_recv.at[array])
 
     def sw_own(array, split, mask):
         return grads[array].at[pl.ds(split * half, half), slab(fs ^ mask)]
@@ -222,13 +220,14 @@
     def sw_copy(array, split, mask):
         order = orders[split]
         phase = first_bit(order, mask)
-        slot = compact(order, mask) - 1
+        place = compact(order, mask)
+        slot, goal = place - 1, place & (place - 1)
         src = sw_own(array, split, mask) if phase == 0 else stages[array].at[split, slot // 2]
         return pltpu.make_async_remote_copy(
             src_ref=src,
             dst_ref=recvs[array].at[split, slot],
-            send_sem=sw_send.at[array, split, slot],
-            recv_sem=sw_recv.at[array, split, slot],
+            send_sem=sw_send.at[array],
+            recv_sem=sw_recv.at[array, split, goal // 2],
             device_id=(fs ^ order[phase], tp),
             device_id_type=MESH,
         )
@@ -237,9 +236,10 @@
         order = orders[split]
         total = sw_own(array, split, mask)[...].astype(F32)
         limit = phases if mask == 0 else first_bit(order, mask)
+        got = recvs[array].at[split, pl.ds(0, limit)]
+        wait_bytes(got, sw_recv.at[array, split, compact(order, mask) // 2])
         for phase in range(limit):
             sent = mask | order[phase]
-            sw_copy(array, split, sent).wait_recv()
             total += recvs[array][split, compact(order, sent) - 1].astype(F32)
         return total
 
@@ -266,8 +266,14 @@
 
     def weight_grad(array, left, right):
         for mask in masks:
-            grads[array][:, slab(fs ^ mask)] = nn(left[...], right[:, slab(fs ^ mask)]).astype(bf16)
+            at = slab(fs ^ mask)
+            halves = array == 2 and mask == masks[0]
+            if not halves:
+                grads[array][:, at] = nn(left[...], right[:, at]).astype(bf16)
             for split in range(2):
+                if halves:
+                    half_rows = pl.ds(split * half, half)
+                    grads[array][half_rows, at] = nn(left[half_rows, :], right[:, at]).astype(bf16)
                 if mask & firsts[split]:
                     sw_copy(array, split, mask).start()
 
@@ -279,8 +285,8 @@
         return pltpu.make_async_remote_copy(
             src_ref=gi.at[g_rows(target, 1 - core, part), :],
             dst_ref=c_buf.at[target, part],
-            send_sem=sc_send.at[target, part],
-            recv_sem=sc_recv.at[target, part],
+            send_sem=sc_send.at[0],
+            recv_sem=sc_recv.at[0],
             device_id=(fs, tp ^ 1),
             device_id_type=MESH,
         )
@@ -295,7 +301,7 @@
         return pltpu.make_async_remote_copy(
             src_ref=c_buf.at[sz_target(way, step), part],
             dst_ref=z_buf.at[way, step, part],
-            send_sem=sz_send.at[way, step, part],
+            send_sem=sz_send.at[way, step],
             recv_sem=sz_recv.at[way, step, part],
             device_id=(fs, tp + CORES if way == 0 else tp - CORES),
             device_id_type=MESH,
@@ -308,7 +314,6 @@
 
     def sc_event(t):
         for part in range(PARTS):
-            sc_copy(t, part).wait_recv()
             c_buf[t, part] = (
                 c_buf[t, part].astype(F32) + gi[g_rows(t, core, part), :].astype(F32)
             ).astype(bf16)
@@ -350,42 +355,30 @@
 
     def g_drain():
         for array in range(2):
-            for part in range(PARTS):
-                gc_copy(array, 0, -1, part).wait_send()
-                for way in range(2):
-                    for step in range(depth - 1):
-
-                        @pl.when(g_sends(way, step))
-                        def _():
-                            gz_copy(array, way, step, part).wait_send()
-
-                        @pl.when(g_arrives(way, step))
-                        def _():
-                            gc_copy(array, way, step, part).wait_send()
-
-        for array in range(3):
-            for split in range(2):
-                order = orders[split]
-                for phase in range(phases):
-                    for index in range(1 << phase):
-                        mask = sum(order[i] for i in range(phase) if index & (1 << i))
-                        gw_copy(array, split, phase, mask).wait_send()
-
-    def sz_drain():
-        for part in range(PARTS):
-            for t in targets:
-                sc_copy(t, part).wait_send()
+            wait_bytes(rows[array].at[pl.ds(0, rows_all // CORES), :], gc_send.at[array])
             for way in range(2):
                 for step in range(depth - 1):
 
-                    @pl.when(s_sends(way, step))
+                    @pl.when(g_sends(way, step))
                     def _():
-                        sz_copy(way, step, part).wait_send()
+                        wait_bytes(rows[array].at[pl.ds(0, n), :], gz_send.at[array, way, step])
+
+        for array in range(3):
+            sent = weights[array].at[:, pl.ds(0, (n_fs - 1) * cols)]
+            wait_bytes(sent, gw_send.at[array])
+
+    def sz_drain():
+        wait_bytes(c_buf, sc_send.at[0])
+        for way in range(2):
+            for step in range(depth - 1):
+
+                @pl.when(s_sends(way, step))
+                def _():
+                    wait_bytes(z_buf.at[way, step], sz_send.at[way, step])
 
     def sw_drain(array):
-        for split in range(2):
-            for mask in range(1, n_fs):
-                sw_copy(array, split, mask).wait_send()
+        sent = grads[array].at[:, pl.ds(0, (n_fs - 1) * cols)]
+        wait_bytes(sent, sw_send.at[array])
 
     tile = min(256, rows_all)
 
@@ -402,7 +395,7 @@
     def up_step(at):
         up_pre = nt(up_full[...], tok_all[at, :])
         gate_pre = act_buf[:, at]
-        sig = jax.nn.sigmoid(gate_pre)
+        sig = 1.0 / (1.0 + jnp.exp(-gate_pre))
         active = gate_pre * sig
         hid_t[:, at] = (active * up_pre).astype(bf16)
         act_buf[:, at] = active
@@ -465,6 +458,7 @@
         for part in range(PARTS):
             sc_copy(t, part).start()
     weight_grad(0, dgate_t, tok_all)
+    wait_bytes(c_buf, sc_recv.at[0])
     for t in targets:
         sc_event(t)
     sz_start()
@@ -514,19 +508,19 @@
             vmem((2, depth - 1, PARTS, sub, width), bf16),
         ]
         + [
-            dma((3, 2, n_fs - 1)),
-            dma((3, 2, n_fs - 1)),
+            dma((3,)),
+            dma((3, 2, n_fs // 2)),
+            dma((2, 2, depth - 1)),
             dma((2, 2, depth - 1, PARTS)),
-            dma((2, 2, depth - 1, PARTS)),
-            dma((2, 2, depth, PARTS)),
-            dma((2, 2, depth, PARTS)),
+            dma((2,)),
+            dma((2,)),
             dma((5,)),
-            dma((3, 2, n_fs - 1)),
-            dma((3, 2, n_fs - 1)),
+            dma((3,)),
+            dma((3, 2, n_fs // 2)),
+            dma((2, depth - 1)),
             dma((2, depth - 1, PARTS)),
-            dma((2, depth - 1, PARTS)),
-            dma((depth, PARTS)),
-            dma((depth, PARTS)),
+            dma((1,)),
+            dma((1,)),
         ]
     )
     return pl.pallas_call(

time: 152 us -> 151 us (level)
  no operation moved by 1% of the time
where the time goes in v4:
time: 151 us; the launch traced here: 150 us
  Pallas kernels  150 us (99%)
    pallas_call x1, Pallas kernels, layer(): pl.pallas_call(functools.partial(layer_kernel, n_fs, n_tp), out_shape=(vm...  147 us

profile of v4, /device:TPU:1, one launch (start us, length us, event | category | flops | bytes accessed | tf_op | source)
XLA Modules:
  0.0 150.3 jit_solution(8888439164843554778)
XLA Ops:
  0.6 147.4 %layer.1 = (bf16[128,2048]{1,0:T(8,128)(2,1)S(1)}, f32[704,512]{1,0:T(8,128)S(1)}, f32[704,512]{1,0:T(8,128)S(1)}, f32[704,512]{1,0:T(8,128)S(1)}) custom-call(bf16[128,2048]{1,0:T(8,128)(2,1)} %refs_0_.1, bf16[704,512]{1,0:T(8,128)(2,1)} %bitcast.4, bf16[704,512]{1,0:T(8,128)(2,1)} %bitcast.5, bf16[704,512]{1,0:T(8,128)(2,1)} %refs_3_.1, ...), custom_call_target="tpu_custom_call" | custom-call | tf_op jit(solution)/shard_map/layer/pallas_call | solution.py:526
  148.0 2.3 %deliver.1 = (bf16[128,2048]{1,0:T(8,128)(2,1)}, f32[704,512]{1,0:T(8,128)}, f32[704,512]{1,0:T(8,128)}, f32[704,512]{1,0:T(8,128)}) custom-call(bf16[128,2048]{1,0:T(8,128)(2,1)S(1)} %get-tuple-element.12.refs_0_, f32[704,512]{1,0:T(8,128)S(1)} %get-tuple-element.13.refs_1_, f32[704,512]{1,0:T(8,128)S(1)} %get-tuple-element.14.refs_2_, ...), custom_call_target="tpu_custom_call" | custom-call | tf_op jit(solution)/shard_map/deliver/pallas_call | solution.py:549

commit v5 on v4

--- a/solution.py
+++ b/solution.py
@@ -101,7 +101,7 @@
     for copy in local:
         copy.start()
     greet(n_fs, depth, fs, tp, z)
-    for copy in local:
+    for copy in local[:2]:
         copy.wait()
 
     def gw_copy(array, split, phase, mask):
@@ -425,6 +425,8 @@
 
     gz_start(TOK)
     gw_start(GATE)
+    for copy in local[2:]:
+        copy.wait()
     gz_event(TOK, 0, 0)
     gw_relays(GATE)
     gw_start(UP)

time: 151 us -> 150 us (level)
  no operation moved by 1% of the time
where the time goes in v5:
time: 150 us
  Pallas kernels  149 us (99%)
    pallas_call x1, Pallas kernels, layer(): pl.pallas_call(functools.partial(layer_kernel, n_fs, n_tp), out_shape=(vm...  147 us

profile of v5, /device:TPU:1, one launch (start us, length us, event | category | flops | bytes accessed | tf_op | source)
XLA Modules:
  0.0 149.5 jit_solution(866093872513938595)
XLA Ops:
  0.6 146.6 %layer.1 = (bf16[128,2048]{1,0:T(8,128)(2,1)S(1)}, f32[704,512]{1,0:T(8,128)S(1)}, f32[704,512]{1,0:T(8,128)S(1)}, f32[704,512]{1,0:T(8,128)S(1)}) custom-call(bf16[128,2048]{1,0:T(8,128)(2,1)} %refs_0_.1, bf16[704,512]{1,0:T(8,128)(2,1)} %bitcast.4, bf16[704,512]{1,0:T(8,128)(2,1)} %bitcast.5, bf16[704,512]{1,0:T(8,128)(2,1)} %refs_3_.1, ...), custom_call_target="tpu_custom_call" | custom-call | tf_op jit(solution)/shard_map/layer/pallas_call | solution.py:528
  147.2 2.3 %deliver.1 = (bf16[128,2048]{1,0:T(8,128)(2,1)}, f32[704,512]{1,0:T(8,128)}, f32[704,512]{1,0:T(8,128)}, f32[704,512]{1,0:T(8,128)}) custom-call(bf16[128,2048]{1,0:T(8,128)(2,1)S(1)} %get-tuple-element.12.refs_0_, f32[704,512]{1,0:T(8,128)S(1)} %get-tuple-element.13.refs_1_, f32[704,512]{1,0:T(8,128)S(1)} %get-tuple-element.14.refs_2_, ...), custom_call_target="tpu_custom_call" | custom-call | tf_op jit(solution)/shard_map/deliver/pallas_call | solution.py:551

commit v6 on v5

--- a/solution.py
+++ b/solution.py
@@ -95,8 +95,8 @@
         pltpu.make_async_copy(ins[0], tok_all.at[own_rows(tp), :], l_sem.at[0]),
         pltpu.make_async_copy(ins[1], gate_full.at[:, slab(fs)], l_sem.at[1]),
         pltpu.make_async_copy(ins[2], up_full.at[:, slab(fs)], l_sem.at[2]),
-        pltpu.make_async_copy(ins[3], down_full.at[:, slab(fs)], l_sem.at[3]),
-        pltpu.make_async_copy(ins[4], cot_all.at[own_rows(tp), :], l_sem.at[4]),
+        pltpu.make_async_copy(ins[3], down_full.at[:, slab(fs)], l_sem.at[2]),
+        pltpu.make_async_copy(ins[4], cot_all.at[own_rows(tp), :], l_sem.at[3]),
     ]
     for copy in local:
         copy.start()
@@ -112,7 +112,7 @@
             src_ref=there,
             dst_ref=there,
             send_sem=gw_send.at[array],
-            recv_sem=gw_recv.at[array, split, min(slot, n_fs // 2 - 1)],
+            recv_sem=gw_recv.at[array, min(slot, n_fs // 2 - 1)],
             device_id=(fs ^ order[phase], tp),
             device_id_type=MESH,
         )
@@ -123,10 +123,11 @@
                 gw_copy(array, split, phase, 0).start()
 
     def gw_event(array, phase, index):
+        slot = (1 << phase) - 1 + index
+        wait_bytes(weights[array].at[:, pl.ds(0, cols)], gw_recv.at[array, slot])
         for split in range(2):
             order = orders[split]
             mask = sum(order[i] for i in range(phase) if index & (1 << i))
-            gw_copy(array, split, phase, mask).wait_recv()
             got = mask | order[phase]
             for later in range(phase + 1, phases):
                 gw_copy(array, split, later, got).start()
@@ -138,10 +139,7 @@
 
     def gw_finish(array):
         last = n_fs // 2
-        for split in range(2):
-            half_rows = pl.ds(split * half, half)
-            landed = weights[array].at[half_rows, pl.ds(0, last * cols)]
-            wait_bytes(landed, gw_recv.at[array, split, last - 1])
+        wait_bytes(weights[array].at[:, pl.ds(0, last * cols)], gw_recv.at[array, last - 1])
 
     def r_block(array, owner, part):
         start = pl.multiple_of(owner * n + part * sub, sub)
@@ -153,7 +151,7 @@
         return pltpu.make_async_remote_copy(
             src_ref=there,
             dst_ref=there,
-            send_sem=gz_send.at[array, way, step],
+            send_sem=gz_send.at[array, way],
             recv_sem=gz_recv.at[array, way, step, part],
             device_id=(fs, tp + sign * CORES),
             device_id_type=MESH,
@@ -227,17 +225,19 @@
             src_ref=src,
             dst_ref=recvs[array].at[split, slot],
             send_sem=sw_send.at[array],
-            recv_sem=sw_recv.at[array, split, goal // 2],
+            recv_sem=sw_recv.at[array, goal // 2],
             device_id=(fs ^ order[phase], tp),
             device_id_type=MESH,
         )
+
+    def sw_wait(array, place):
+        limit = phases if place == 0 else (place & -place).bit_length() - 1
+        wait_bytes(recvs[array].at[:, pl.ds(0, limit)], sw_recv.at[array, place // 2])
 
     def sw_sum(array, split, mask):
         order = orders[split]
         total = sw_own(array, split, mask)[...].astype(F32)
         limit = phases if mask == 0 else first_bit(order, mask)
-        got = recvs[array].at[split, pl.ds(0, limit)]
-        wait_bytes(got, sw_recv.at[array, split, compact(order, mask) // 2])
         for phase in range(limit):
             sent = mask | order[phase]
             total += recvs[array][split, compact(order, sent) - 1].astype(F32)
@@ -248,6 +248,7 @@
 
     def sw_relay(array):
         for mask in later:
+            sw_wait(array, mask)
             for split in range(2):
                 order = orders[split]
                 real = sum(bit for i, bit in enumerate(order) if mask & (1 << i))
@@ -256,6 +257,7 @@
                 sw_copy(array, split, real).start()
 
     def sw_finish(array):
+        sw_wait(array, 0)
         for split in range(2):
             w_res[array][pl.ds(split * half, half), :] = sw_sum(array, split, 0)
 
@@ -301,7 +303,7 @@
         return pltpu.make_async_remote_copy(
             src_ref=c_buf.at[sz_target(way, step), part],
             dst_ref=z_buf.at[way, step, part],
-            send_sem=sz_send.at[way, step],
+            send_sem=sz_send.at[way],
             recv_sem=sz_recv.at[way, step, part],
             device_id=(fs, tp + CORES if way == 0 else tp - CORES),
             device_id_type=MESH,
@@ -357,11 +359,11 @@
         for array in range(2):
             wait_bytes(rows[array].at[pl.ds(0, rows_all // CORES), :], gc_send.at[array])
             for way in range(2):
-                for step in range(depth - 1):
-
-                    @pl.when(g_sends(way, step))
+                for count in range(1, depth):
+
+                    @pl.when((z if way == 0 else depth - 1 - z) == count - 1)
                     def _():
-                        wait_bytes(rows[array].at[pl.ds(0, n), :], gz_send.at[array, way, step])
+                        wait_bytes(rows[array].at[pl.ds(0, count * n), :], gz_send.at[array, way])
 
         for array in range(3):
             sent = weights[array].at[:, pl.ds(0, (n_fs - 1) * cols)]
@@ -370,11 +372,11 @@
     def sz_drain():
         wait_bytes(c_buf, sc_send.at[0])
         for way in range(2):
-            for step in range(depth - 1):
-
-                @pl.when(s_sends(way, step))
+            for count in range(1, depth):
+
+                @pl.when(sz_from(way) == depth - 1 - count)
                 def _():
-                    wait_bytes(z_buf.at[way, step], sz_send.at[way, step])
+                    wait_bytes(z_buf.at[way, pl.ds(0, count)], sz_send.at[way])
 
     def sw_drain(array):
         sent = grads[array].at[:, pl.ds(0, (n_fs - 1) * cols)]
@@ -425,8 +427,8 @@
 
     gz_start(TOK)
     gw_start(GATE)
-    for copy in local[2:]:
-        copy.wait()
+    wait_bytes(up_full.at[:, pl.ds(0, 2 * cols)], l_sem.at[2])
+    local[4].wait()
     gz_event(TOK, 0, 0)
     gw_relays(GATE)
     gw_start(UP)
@@ -511,15 +513,15 @@
         ]
         + [
             dma((3,)),
-            dma((3, 2, n_fs // 2)),
-            dma((2, 2, depth - 1)),
+            dma((3, n_fs // 2)),
+            dma((2, 2)),
             dma((2, 2, depth - 1, PARTS)),
             dma((2,)),
             dma((2,)),
-            dma((5,)),
+            dma((4,)),
             dma((3,)),
-            dma((3, 2, n_fs // 2)),
-            dma((2, depth - 1)),
+            dma((3, n_fs // 2)),
+            dma((2,)),
             dma((2, depth - 1, PARTS)),
             dma((1,)),
             dma((1,)),

time: 150 us -> 149 us (level)
  no operation moved by 1% of the time
where the time goes in v6:
time: 149 us
  Pallas kernels  149 us (100%)
    pallas_call x1, Pallas kernels, layer(): pl.pallas_call(functools.partial(layer_kernel, n_fs, n_tp), out_shape=(vm...  146 us

profile of v6, /device:TPU:1, one launch (start us, length us, event | category | flops | bytes accessed | tf_op | source)
XLA Modules:
  0.0 149.3 jit_solution(15138138501413014713)
XLA Ops:
  0.6 146.4 %layer.1 = (bf16[128,2048]{1,0:T(8,128)(2,1)S(1)}, f32[704,512]{1,0:T(8,128)S(1)}, f32[704,512]{1,0:T(8,128)S(1)}, f32[704,512]{1,0:T(8,128)S(1)}) custom-call(bf16[128,2048]{1,0:T(8,128)(2,1)} %refs_0_.1, bf16[704,512]{1,0:T(8,128)(2,1)} %bitcast.4, bf16[704,512]{1,0:T(8,128)(2,1)} %bitcast.5, bf16[704,512]{1,0:T(8,128)(2,1)} %refs_3_.1, ...), custom_call_target="tpu_custom_call" | custom-call | tf_op jit(solution)/shard_map/layer/pallas_call | solution.py:530
  147.0 2.3 %deliver.1 = (bf16[128,2048]{1,0:T(8,128)(2,1)}, f32[704,512]{1,0:T(8,128)}, f32[704,512]{1,0:T(8,128)}, f32[704,512]{1,0:T(8,128)}) custom-call(bf16[128,2048]{1,0:T(8,128)(2,1)S(1)} %get-tuple-element.12.refs_0_, f32[704,512]{1,0:T(8,128)S(1)} %get-tuple-element.13.refs_1_, f32[704,512]{1,0:T(8,128)S(1)} %get-tuple-element.14.refs_2_, ...), custom_call_target="tpu_custom_call" | custom-call | tf_op jit(solution)/shard_map/deliver/pallas_call | solution.py:553

commit v7 on v6

--- a/solution.py
+++ b/solution.py
@@ -62,13 +62,14 @@
 
 
 def layer_kernel(n_fs, n_tp, *refs):
-    ins, outs, scratch = refs[:5], refs[5:9], refs[9:]
+    ins, outs, scratch = refs[:5], refs[5:10], refs[10:]
     tok_all, cot_all, gate_full, up_full, down_full = scratch[:5]
     act_buf, fac_buf, hid_t, dgate_t, dup_t, dgate, dup = scratch[5:12]
-    grads, recvs, stages = scratch[12:15], scratch[15:18], scratch[18:21]
-    gi, c_buf, z_buf = scratch[21:24]
-    gw_send, gw_recv, gz_send, gz_recv, gc_send, gc_recv, l_sem = scratch[24:31]
-    sw_send, sw_recv, sz_send, sz_recv, sc_send, sc_recv = scratch[31:]
+    grads, recvs, stages = scratch[12:14], scratch[14:16], scratch[16:19]
+    grads, recvs = (grads[0], outs[3], grads[1]), (recvs[0], outs[4], recvs[1])
+    gi, c_buf, z_buf = scratch[19:22]
+    gw_send, gw_recv, gz_send, gz_recv, gc_send, gc_recv, l_sem = scratch[22:29]
+    sw_send, sw_recv, sz_send, sz_recv, sc_send, sc_recv = scratch[29:]
     fs, tp = lax.axis_index("fs"), lax.axis_index("tp")
     depth = n_tp // CORES
     z, core = tp // CORES, tp % CORES
@@ -83,7 +84,7 @@
     sub = n // PARTS
     rows = (tok_all, cot_all)
     weights = (gate_full, up_full, down_full)
-    gi_res, *w_res = outs
+    gi_res, w_res = outs[0], (outs[1], None, outs[2])
 
     def slab(owner):
         return pl.ds(pl.multiple_of(owner * cols, cols), cols)
@@ -480,7 +481,7 @@
     sz_finish()
     sz_drain()
     sw_finish(0)
-    sw_finish(1)
+    sw_wait(1, 0)
 
     sw_drain(0)
     sw_drain(1)
@@ -503,8 +504,8 @@
         + [vmem((ff, rows_all), F32)] * 2
         + [vmem((ff, rows_all), bf16)] * 3
         + [vmem((rows_all, ff), bf16)] * 2
-        + [vmem((ff, width), bf16)] * 3
-        + [vmem((2, n_fs - 1, half, cols), bf16)] * 3
+        + [vmem((ff, width), bf16)] * 2
+        + [vmem((2, n_fs - 1, half, cols), bf16)] * 2
         + [vmem((2, n_stage, half, cols), bf16)] * 3
         + [
             vmem((rows_all, width), bf16),
@@ -529,41 +530,59 @@
     )
     return pl.pallas_call(
         functools.partial(layer_kernel, n_fs, n_tp),
-        out_shape=(vmem((n, width), bf16),) + (vmem((ff, cols), F32),) * 3,
+        out_shape=(vmem((n, width), bf16),)
+        + (vmem((ff, cols), F32),) * 2
+        + (vmem((ff, width), bf16), vmem((2, n_fs - 1, half, cols), bf16)),
         in_specs=[hbm] * 5,
-        out_specs=[pl.BlockSpec(memory_space=vmem)] * 4,
+        out_specs=[pl.BlockSpec(memory_space=vmem)] * 5,
         scratch_shapes=scratch,
         compiler_params=pltpu.CompilerParams(
-            collective_id=0, has_side_effects=True, vmem_limit_bytes=61000000
+            collective_id=0, has_side_effects=True, vmem_limit_bytes=57000000
         ),
         name="layer",
     )(tokens, gate, up, down, cot)
 
 
-def deliver_kernel(*refs):
-    ins, outs, sem = refs[:4], refs[4:8], refs[8]
-    copies = [pltpu.make_async_copy(a, b, sem.at[i]) for i, (a, b) in enumerate(zip(ins, outs))]
+def deliver_kernel(n_fs, *refs):
+    gi, gate, down, own, got = refs[:5]
+    outs, total, sem = refs[5:9], refs[9], refs[10]
+    half, cols = got.shape[2:]
+    fs = lax.axis_index("fs")
+    slab = pl.ds(pl.multiple_of(fs * cols, cols), cols)
+    copies = [
+        pltpu.make_async_copy(a, outs[i], sem.at[i]) for a, i in ((gi, 0), (gate, 1), (down, 3))
+    ]
     for copy in copies:
         copy.start()
+    for split in range(2):
+        at = pl.ds(split * half, half)
+        summed = own[at, slab].astype(F32)
+        for phase in range(n_fs.bit_length() - 1):
+            summed += got[split, (1 << phase) - 1].astype(F32)
+        total[at, :] = summed
+        copies.append(pltpu.make_async_copy(total.at[at, :], outs[2].at[at, :], sem.at[4 + split]))
+        copies[-1].start()
     for copy in copies:
         copy.wait()
 
 
-def deliver(*arrays):
+def deliver(n_fs, gi, gate, down, own, got):
+    vmem = pltpu.VMEM
+    shapes = [jax.ShapeDtypeStruct(a.shape, a.dtype) for a in (gi, gate, gate, down)]
     return pl.pallas_call(
-        deliver_kernel,
-        out_shape=tuple(jax.ShapeDtypeStruct(a.shape, a.dtype) for a in arrays),
-        in_specs=[pl.BlockSpec(memory_space=pltpu.VMEM)] * 4,
+        functools.partial(deliver_kernel, n_fs),
+        out_shape=tuple(shapes),
+        in_specs=[pl.BlockSpec(memory_space=vmem)] * 5,
         out_specs=[pl.BlockSpec(memory_space=pl.ANY)] * 4,
-        scratch_shapes=[pltpu.SemaphoreType.DMA((4,))],
-        compiler_params=pltpu.CompilerParams(vmem_limit_bytes=1 << 20),
+        scratch_shapes=[vmem(gate.shape, F32), pltpu.SemaphoreType.DMA((6,))],
+        compiler_params=pltpu.CompilerParams(vmem_limit_bytes=2 << 20),
         name="deliver",
-    )(*arrays)
+    )(gi, gate, down, own, got)
 
 
 def body(n_fs, n_tp, tokens, gate_weight, up_weight, down_weight, grad_out):
     results = layer(n_fs, n_tp, tokens, gate_weight.T, up_weight.T, down_weight, grad_out)
-    grad_input, grad_gate, grad_up, grad_down = deliver(*results)
+    grad_input, grad_gate, grad_up, grad_down = deliver(n_fs, *results)
     return grad_input, grad_gate.T, grad_up.T, grad_down
 
 

time: 149 us -> 149 us (level)
  no operation moved by 1% of the time
where the time goes in v7:
time: 149 us
  Pallas kernels  148 us (99%)
    pallas_call x1, Pallas kernels, layer(): pl.pallas_call(functools.partial(layer_kernel, n_fs, n_tp), out_shape=(vm...  146 us

profile of v7, /device:TPU:1, one launch (start us, length us, event | category | flops | bytes accessed | tf_op | source)
XLA Modules:
  0.0 149.1 jit_solution(2014202881785832090)
XLA Ops:
  0.6 146.1 %layer.1 = (bf16[128,2048]{1,0:T(8,128)(2,1)S(1)}, f32[704,512]{1,0:T(8,128)S(1)}, f32[704,512]{1,0:T(8,128)S(1)}, bf16[704,2048]{1,0:T(8,128)(2,1)S(1)}, bf16[2,3,352,512]{3,2,1,0:T(8,128)(2,1)S(1)}) custom-call(bf16[128,2048]{1,0:T(8,128)(2,1)} %refs_0_.1, bf16[704,512]{1,0:T(8,128)(2,1)} %bitcast.4, bf16[704,512]{1,0:T(8,128)(2,1)} %bitcast.5, ...), custom_call_target="tpu_custom_call" | custom-call | tf_op jit(solution)/shard_map/layer/pallas_call | solution.py:531
  146.8 2.3 %deliver.1 = (bf16[128,2048]{1,0:T(8,128)(2,1)}, f32[704,512]{1,0:T(8,128)}, f32[704,512]{1,0:T(8,128)}, f32[704,512]{1,0:T(8,128)}) custom-call(bf16[128,2048]{1,0:T(8,128)(2,1)S(1)} %get-tuple-element.13.refs_0_, f32[704,512]{1,0:T(8,128)S(1)} %get-tuple-element.14.refs_1_, f32[704,512]{1,0:T(8,128)S(1)} %get-tuple-element.15.refs_2_, ...), custom_call_target="tpu_custom_call" | custom-call | tf_op jit(solution)/shard_map/deliver/pallas_call | solution.py:572

commit v8 on v7

--- a/solution.py
+++ b/solution.py
@@ -10,6 +10,7 @@
 MESH = pl.DeviceIdType.MESH
 CORES = 2
 PARTS = 2
+SUM_PARTS = 1
 F32 = jnp.float32
 
 
@@ -82,6 +83,7 @@
     cols = width // n_fs
     half = ff // 2
     sub = n // PARTS
+    piece = n // SUM_PARTS
     rows = (tok_all, cot_all)
     weights = (gate_full, up_full, down_full)
     gi_res, w_res = outs[0], (outs[1], None, outs[2])
@@ -281,8 +283,8 @@
                     sw_copy(array, split, mask).start()
 
     def g_rows(target, which, part):
-        start = (target * CORES + which) * n + part * sub
-        return pl.ds(pl.multiple_of(start, sub), sub)
+        start = (target * CORES + which) * n + part * piece
+        return pl.ds(pl.multiple_of(start, piece), piece)
 
     def sc_copy(target, part):
         return pltpu.make_async_remote_copy(
@@ -316,14 +318,14 @@
     targets = [depth - 1 - i // 2 if i % 2 == 0 else i // 2 for i in range(depth)]
 
     def sc_event(t):
-        for part in range(PARTS):
+        for part in range(SUM_PARTS):
             c_buf[t, part] = (
                 c_buf[t, part].astype(F32) + gi[g_rows(t, core, part), :].astype(F32)
             ).astype(bf16)
 
     def sz_start():
         for step in range(depth - 1):
-            for part in range(PARTS):
+            for part in range(SUM_PARTS):
                 for way in range(2):
 
                     @pl.when(sz_from(way) == 0)
@@ -347,14 +349,14 @@
                     sz_copy(way, step, part).start()
 
     def sz_finish():
-        zero = jnp.zeros((sub, width), F32)
-        for part in range(PARTS):
+        zero = jnp.zeros((piece, width), F32)
+        for part in range(SUM_PARTS):
             total = c_buf[z, part].astype(F32)
             from_left = z_buf[0, jnp.clip(depth - 1 - z, 0, depth - 2), part].astype(F32)
             from_right = z_buf[1, jnp.clip(z, 0, depth - 2), part].astype(F32)
             total += jnp.where(z > 0, from_left, zero)
             total += jnp.where(z < depth - 1, from_right, zero)
-            gi_res[pl.ds(part * sub, sub), :] = total.astype(bf16)
+            gi_res[pl.ds(part * piece, piece), :] = total.astype(bf16)
 
     def g_drain():
         for array in range(2):
@@ -460,7 +462,7 @@
     sw_relay(2)
     gi_steps(gi_count // 2, gi_count)
     for t in targets:
-        for part in range(PARTS):
+        for part in range(SUM_PARTS):
             sc_copy(t, part).start()
     weight_grad(0, dgate_t, tok_all)
     wait_bytes(c_buf, sc_recv.at[0])
@@ -472,7 +474,7 @@
     sw_finish(2)
     sw_drain(2)
     for hop in range(1, depth):
-        for part in range(PARTS):
+        for part in range(SUM_PARTS):
             sz_event(hop, part)
         if hop == 1:
             sw_relay(0)
@@ -496,7 +498,7 @@
     hbm = pl.BlockSpec(memory_space=pl.ANY)
     vmem = pltpu.VMEM
     dma = pltpu.SemaphoreType.DMA
-    half, sub = ff // 2, n // PARTS
+    half = ff // 2
     n_stage = max(n_fs // 2 - 1, 1)
     scratch = (
         [vmem((rows_all, width), bf16)] * 2
@@ -509,8 +511,8 @@
         + [vmem((2, n_stage, half, cols), bf16)] * 3
         + [
             vmem((rows_all, width), bf16),
-            vmem((depth, PARTS, sub, width), bf16),
-            vmem((2, depth - 1, PARTS, sub, width), bf16),
+            vmem((depth, SUM_PARTS, n // SUM_PARTS, width), bf16),
+            vmem((2, depth - 1, SUM_PARTS, n // SUM_PARTS, width), bf16),
         ]
         + [
             dma((3,)),
@@ -523,7 +525,7 @@
             dma((3,)),
             dma((3, n_fs // 2)),
             dma((2,)),
-            dma((2, depth - 1, PARTS)),
+            dma((2, depth - 1, SUM_PARTS)),
             dma((1,)),
             dma((1,)),
         ]

time: 149 us -> 149 us (level)
  no operation moved by 1% of the time
where the time goes in v8:
time: 149 us
  Pallas kernels  148 us (99%)
    pallas_call x1, Pallas kernels, layer(): pl.pallas_call(functools.partial(layer_kernel, n_fs, n_tp), out_shape=(vm...  146 us

profile of v8, /device:TPU:1, one launch (start us, length us, event | category | flops | bytes accessed | tf_op | source)
XLA Modules:
  0.0 149.0 jit_solution(8535076865852735483)
XLA Ops:
  0.6 146.1 %layer.1 = (bf16[128,2048]{1,0:T(8,128)(2,1)S(1)}, f32[704,512]{1,0:T(8,128)S(1)}, f32[704,512]{1,0:T(8,128)S(1)}, bf16[704,2048]{1,0:T(8,128)(2,1)S(1)}, bf16[2,3,352,512]{3,2,1,0:T(8,128)(2,1)S(1)}) custom-call(bf16[128,2048]{1,0:T(8,128)(2,1)} %refs_0_.1, bf16[704,512]{1,0:T(8,128)(2,1)} %bitcast.4, bf16[704,512]{1,0:T(8,128)(2,1)} %bitcast.5, ...), custom_call_target="tpu_custom_call" | custom-call | tf_op jit(solution)/shard_map/layer/pallas_call | solution.py:533
  146.7 2.3 %deliver.1 = (bf16[128,2048]{1,0:T(8,128)(2,1)}, f32[704,512]{1,0:T(8,128)}, f32[704,512]{1,0:T(8,128)}, f32[704,512]{1,0:T(8,128)}) custom-call(bf16[128,2048]{1,0:T(8,128)(2,1)S(1)} %get-tuple-element.13.refs_0_, f32[704,512]{1,0:T(8,128)S(1)} %get-tuple-element.14.refs_1_, f32[704,512]{1,0:T(8,128)S(1)} %get-tuple-element.15.refs_2_, ...), custom_call_target="tpu_custom_call" | custom-call | tf_op jit(solution)/shard_map/deliver/pallas_call | solution.py:574
